TPU v7x, 32 devices: a whole 2x2x4 slice. The times are simulated.
32 devices in a mesh: sp: 4 (over z), dp: 8 (over y, x, core).
Axes of the slice: x: 2, y: 2, z: 4, core: 2. Of those that a mesh axis runs over, the one named last changes fastest.
Arguments:
- inputs: bfloat16 [8, 512, 2048], P('dp', 'sp'), may hold values from -6 to 6
- queries: bfloat16 [8, 512, 1024], P('dp', 'sp'), may hold values from -6 to 6
- keys: bfloat16 [8, 512, 1024], P('dp', 'sp'), may hold values from -1.5 to 1.5
- values: bfloat16 [8, 512, 1024], P('dp', 'sp'), may hold values from -6 to 6
- log_decay: bfloat16 [8, 512, 1024], P('dp', 'sp'), may hold values from -0.1 to 0, as said below
- cotangent: bfloat16 [8, 512, 1024], P('dp', 'sp'), may hold values from -0.59765625 to 0.59765625
- value_weight: bfloat16 [2048, 1024], P('dp'), may hold values from -0.125 to 0.125
Outputs:
- grad_queries: bfloat16 [8, 512, 1024], P('dp', 'sp')
- grad_keys: bfloat16 [8, 512, 1024], P('dp', 'sp')
- grad_decay: bfloat16 [8, 512, 1024], P('dp', 'sp')
- grad_inputs: bfloat16 [8, 512, 2048], P('dp', 'sp')
- grad_weight: float32 [2048, 1024], P('dp')
Inputs may be any that keep to these rules, and one draw needn't show every extreme that they name: `log_decay`: the log decays are negative; per key channel and sequence they differ between positions.
All inputs are finite; a program needn't handle non-finite values.
Results may differ from a plain program's by a relative error of at most 0.015.
Values may be sent and summed in bfloat16 or wider, within the bound.
No kernel may reach another device: no remote copies, remote signals or barrier semaphores. Data moves between devices by JAX's collectives and lax.ppermute only.
A program may use at most 128 MiB of HBM per device.

v0:
```python
import functools

import jax
import jax.numpy as jnp
from jax import lax
from jax.experimental import pallas as pl
from jax.experimental.pallas import tpu as pltpu
from jax.sharding import PartitionSpec as P

HEAD_DIM = 64
PAIR = 2 * HEAD_DIM
SCALE = HEAD_DIM ** (-0.5)
BF = jnp.bfloat16
F32 = jnp.float32


def dot(a, b, ca, cb):
    return lax.dot_general(a, b, (((ca,), (cb,)), ((), ())), preferred_element_type=F32)


def iotas(rows, cols):
    return (
        lax.broadcasted_iota(jnp.int32, (rows, cols), 0),
        lax.broadcasted_iota(jnp.int32, (rows, cols), 1),
    )


def first_head(rows):
    return iotas(rows, PAIR)[1] < HEAD_DIM


def running_sums(gate):
    length = gate.shape[0]
    row, col = iotas(length, length)
    running = dot((row >= col).astype(BF), gate, 1, 0)
    return running, running - gate.astype(F32), running[length - 1 : length]


def pack(full):
    return jnp.where(first_head(HEAD_DIM), full[:HEAD_DIM], full[HEAD_DIM:])


def unpack(state):
    mine = first_head(HEAD_DIM)
    zero = jnp.zeros_like(state)
    return jnp.concatenate([jnp.where(mine, state, zero), jnp.where(mine, zero, state)], axis=0)


def both_heads(rows):
    mine = first_head(rows.shape[0])
    zero = jnp.zeros_like(rows)
    return jnp.where(mine, rows, zero), jnp.where(mine, zero, rows)


def lanes(pair):
    return slice(pair * PAIR, (pair + 1) * PAIR)


def state_rows(pair):
    return slice(pair * HEAD_DIM, (pair + 1) * HEAD_DIM)


def read_states_kernel(place, q_ref, g_ref, o_ref, *out, pairs, seq_devices):
    me = place[0]
    high, low = [], []
    for pair in range(pairs):
        at = lanes(pair)
        running, exclusive, total = running_sums(g_ref[:, at])
        query = q_ref[:, at].astype(F32) * SCALE
        both = jnp.concatenate(
            [
                (query * jnp.exp(running)).astype(BF),
                (query * jnp.exp(total - exclusive)).astype(BF),
            ],
            axis=1,
        )
        full = dot(o_ref[:, at], both, 0, 0)
        to_earlier = pack(full[:, :PAIR]).astype(BF)
        to_later = pack(full[:, PAIR:]).astype(BF)
        for shift in range(1, seq_devices):
            later = jnp.full((HEAD_DIM, PAIR), me + shift, jnp.int32) < seq_devices
            out[shift - 1][state_rows(pair), :] = jnp.where(
                later, to_later.astype(F32), to_earlier.astype(F32)
            ).astype(BF)
        decay = jnp.exp(total)
        top = decay.astype(BF).astype(F32)
        high.append(top)
        low.append(decay - top)
    decays = jnp.concatenate(high + low, axis=0).astype(BF)
    for shift in range(1, seq_devices):
        out[shift - 1][pairs * HEAD_DIM :, :] = decays


def inner_values_kernel(place, q_ref, k_ref, v_ref, g_ref, o_ref, *out, pairs, seq_devices):
    me = place[0]
    inner_ref = out[0]
    length = q_ref.shape[0]
    row, col = iotas(length, length)
    for pair in range(pairs):
        at = lanes(pair)
        running, exclusive, total = running_sums(g_ref[:, at])
        query = q_ref[:, at].astype(F32) * SCALE
        key = k_ref[:, at].astype(F32)
        query_fwd = (query * jnp.exp(running)).astype(BF)
        query_bwd = (query * jnp.exp(-exclusive)).astype(BF)
        key_fwd = both_heads((key * jnp.exp(-running)).astype(BF))
        key_late = (key * jnp.exp(exclusive)).astype(BF)
        key_bwd = both_heads(key_late)
        key_end = (key * jnp.exp(total - running)).astype(BF)
        scores = []
        for head in range(2):
            ahead = dot(key_fwd[head], query_fwd, 1, 1)
            behind = dot(key_bwd[head], query_bwd, 1, 1)
            scores.append(
                (jnp.where(row <= col, ahead, 0.0) + jnp.where(row >= col, behind, 0.0)).astype(BF)
            )
        upstream = o_ref[:, at]
        inner_ref[:, at] = dot(
            jnp.concatenate(scores, axis=1), jnp.concatenate(both_heads(upstream), axis=0), 1, 0
        )
        full = dot(v_ref[:, at], jnp.concatenate([key_end, key_late], axis=1), 0, 0)
        to_later = pack(full[:, :PAIR])
        to_earlier = pack(full[:, PAIR:])
        for shift in range(1, seq_devices):
            later = jnp.full((HEAD_DIM, PAIR), me + shift, jnp.int32) < seq_devices
            out[shift][state_rows(pair), :] = jnp.where(later, to_later, to_earlier).astype(BF)


def gather_states(me, messages, decays, pair, seq_devices):
    before = jnp.zeros((HEAD_DIM, PAIR), F32)
    after = jnp.zeros((HEAD_DIM, PAIR), F32)
    weight_before = jnp.ones((1, PAIR), F32)
    weight_after = jnp.ones((1, PAIR), F32)

    def state(shift):
        return messages[shift - 1][state_rows(pair), :].astype(F32)

    for shift in range(1, seq_devices):
        earlier = jnp.full((HEAD_DIM, PAIR), me, jnp.int32) >= shift
        before = before + jnp.where(earlier, weight_before * state(shift), 0.0)
        weight_before = weight_before * decays(shift)
    for shift in range(seq_devices - 1, 0, -1):
        later = jnp.full((HEAD_DIM, PAIR), me, jnp.int32) < shift
        after = after + jnp.where(later, weight_after * state(shift), 0.0)
        weight_after = weight_after * decays(shift)
    return before, after


def decay_reader(messages, pair, pairs):
    base = pairs * HEAD_DIM

    def decays(shift):
        tail = messages[shift - 1][base : base + 2 * pairs, :].astype(F32)
        return tail[pair : pair + 1] + tail[pairs + pair : pairs + pair + 1]

    return decays


def values_kernel(place, k_ref, g_ref, inner_ref, *rest, pairs, seq_devices):
    me = place[0]
    messages = rest[: seq_devices - 1]
    value_ref, before_ref, after_ref = rest[seq_devices - 1 :]
    width = value_ref.shape[2]
    for pair in range(pairs):
        at = lanes(pair)
        running, exclusive, total = running_sums(g_ref[:, at])
        key = k_ref[:, at].astype(F32)
        before, after = gather_states(
            me, messages, decay_reader(messages, pair, pairs), pair, seq_devices
        )
        before_ref[state_rows(pair), :] = before
        after_ref[state_rows(pair), :] = after
        keys = jnp.concatenate(
            [
                (key * jnp.exp(total - running)).astype(BF),
                (key * jnp.exp(exclusive)).astype(BF),
            ],
            axis=1,
        )
        states = jnp.concatenate([unpack(after), unpack(before)], axis=1).astype(BF)
        grad = (inner_ref[:, at] + dot(keys, states, 1, 1)).astype(BF)
        step = min(width, PAIR)
        for start in range(0, PAIR, step):
            block, offset = divmod(pair * PAIR + start, width)
            value_ref[block, :, offset : offset + step] = grad[:, start : start + step]


def rest_kernel(place, q_ref, k_ref, v_ref, g_ref, o_ref, before_ref, after_ref, *rest, pairs, seq_devices):
    me = place[0]
    count = seq_devices - 1
    read_messages = rest[:count]
    write_messages = rest[count : 2 * count]
    gq_ref, gk_ref, gg_ref = rest[2 * count :]
    length = q_ref.shape[0]
    row, col = iotas(length, length)
    tail = (row <= col).astype(BF)
    for pair in range(pairs):
        at = lanes(pair)
        running, exclusive, total = running_sums(g_ref[:, at])
        query = q_ref[:, at].astype(F32)
        key = k_ref[:, at].astype(F32)
        value = v_ref[:, at]
        upstream = o_ref[:, at]
        grow_run = jnp.exp(running)
        shrink_run = jnp.exp(-running)
        grow_exc = jnp.exp(exclusive)
        shrink_exc = jnp.exp(-exclusive)
        end = jnp.exp(total)
        query_fwd = query * (SCALE * grow_run)
        query_bwd = query * (SCALE * shrink_exc)
        key_fwd = key * shrink_run
        key_bwd = key * grow_exc
        read_before = before_ref[state_rows(pair), :]
        read_after = after_ref[state_rows(pair), :]
        before, after = gather_states(
            me, write_messages, decay_reader(read_messages, pair, pairs), pair, seq_devices
        )
        write_own = pack(dot(value, (key * jnp.exp(total - running)).astype(BF), 0, 0))
        read_own = pack(
            dot(upstream, (query * (SCALE * jnp.exp(total - exclusive))).astype(BF), 0, 0)
        )
        through = jnp.sum(
            (end * before + write_own) * read_after + (end * read_before + read_own) * after,
            axis=0,
            keepdims=True,
        )
        value_heads = both_heads(value)
        upstream_heads = both_heads(upstream)
        low, high, low_turned, high_turned = [], [], [], []
        for head in range(2):
            product = dot(upstream_heads[head], value, 1, 1)
            turned = dot(value_heads[head], upstream, 1, 1)
            low.append(jnp.where(row >= col, product, 0.0).astype(BF))
            high.append(jnp.where(row <= col, product, 0.0).astype(BF))
            low_turned.append(jnp.where(row <= col, turned, 0.0).astype(BF))
            high_turned.append(jnp.where(row >= col, turned, 0.0).astype(BF))

        def total_of(blocks, outer, rows, state):
            left = jnp.concatenate(blocks + [outer], axis=1)
            right = jnp.concatenate(both_heads(rows.astype(BF)) + (unpack(state).astype(BF),), axis=0)
            return dot(left, right, 1, 0)

        gq_fwd = total_of(low, upstream, key_fwd, before) * (SCALE * grow_run)
        gq_bwd = total_of(high, upstream, key_bwd, after * end) * (SCALE * shrink_exc)
        gk_fwd = total_of(low_turned, value, query_fwd, read_after * end) * shrink_run
        gk_bwd = total_of(high_turned, value, query_bwd, read_before) * grow_exc
        gq_ref[:, at] = (gq_fwd + gq_bwd).astype(BF)
        gk_ref[:, at] = (gk_fwd + gk_bwd).astype(BF)
        backward = key * gk_bwd - query * gq_bwd
        change = query * gq_fwd - key * gk_fwd + backward
        top = change.astype(BF)
        bottom = (change - top.astype(F32)).astype(BF)
        summed = dot(tail, jnp.concatenate([top, bottom], axis=1), 1, 0)
        gg_ref[:, at] = (summed[:, :PAIR] + summed[:, PAIR:] - backward + through).astype(BF)


def source_of(place, step, row_devices):
    chips = row_devices // 2
    mine = place[1]
    core = lax.rem(mine, 2)
    chip = lax.rem(lax.div(mine, 2) + chips - step // 2, chips)
    return 2 * chip + (core if step % 2 == 0 else 1 - core)


def weight_kernel(place, x_ref, *rest, row_devices):
    pieces = rest[:row_devices]
    out_ref = rest[row_devices]
    for block in range(out_ref.shape[0]):
        acc = jnp.zeros(out_ref.shape[1:], F32)
        for step in range(row_devices):
            acc = acc + dot(x_ref[source_of(place, step, row_devices)], pieces[step][block], 1, 0)
        out_ref[block] = acc.astype(BF)


def inputs_kernel(place, w_ref, *rest, row_devices):
    pieces = rest[:row_devices]
    out_ref = rest[row_devices]
    blocks, _, width = pieces[0].shape
    for step in range(row_devices):
        acc = jnp.zeros(out_ref.shape[1:], F32)
        for block in range(blocks):
            acc = acc + dot(pieces[step][block], w_ref[:, block * width : (block + 1) * width], 1, 1)
        out_ref[source_of(place, step, row_devices)] = acc.astype(BF)


def call(body, shapes, place, *operands, name):
    specs = [pl.BlockSpec(memory_space=pltpu.SMEM)] + [
        pl.BlockSpec(memory_space=pltpu.VMEM) for _ in operands
    ]
    return pl.pallas_call(
        body,
        out_shape=[jax.ShapeDtypeStruct(shape, dtype) for shape, dtype in shapes],
        in_specs=specs,
        out_specs=[pl.BlockSpec(memory_space=pltpu.VMEM) for _ in shapes],
        name=name,
    )(place, *operands)


def per_device(inputs, queries, keys, values, log_decay, cotangent, value_weight):
    seq_devices = lax.axis_size("sp")
    row_devices = lax.axis_size("dp")
    chips = row_devices // 2
    tokens, width = queries.shape[1:]
    pairs = width // PAIR
    rows = value_weight.shape[0]
    columns = width // seq_devices
    place = jnp.stack([lax.axis_index("sp"), lax.axis_index("dp")]).astype(jnp.int32)
    query, key, value, gate, upstream = (
        array[0] for array in (queries, keys, values, log_decay, cotangent)
    )
    sizes = dict(pairs=pairs, seq_devices=seq_devices)
    count = seq_devices - 1

    def around(messages):
        return [
            lax.ppermute(
                message, "sp", [(i, (i + shift) % seq_devices) for i in range(seq_devices)]
            )
            for shift, message in enumerate(messages, 1)
        ]

    read_own = call(
        functools.partial(read_states_kernel, **sizes),
        [((pairs * HEAD_DIM + 2 * pairs, PAIR), BF)] * count,
        place, query, gate, upstream, name="read_states",
    )
    read_other = around(read_own)
    inner, *write_own = call(
        functools.partial(inner_values_kernel, **sizes),
        [((tokens, width), F32)] + [((pairs * HEAD_DIM, PAIR), BF)] * count,
        place, query, key, value, gate, upstream, name="inner_values",
    )
    input_rows = lax.all_to_all(
        inputs[0].reshape(tokens, row_devices, rows).transpose(1, 2, 0), "dp", 0, 0, tiled=True
    )
    value_grad, before, after = call(
        functools.partial(values_kernel, **sizes),
        [((seq_devices, tokens, columns), BF)] + [((pairs * HEAD_DIM, PAIR), F32)] * 2,
        place, key, gate, inner, *read_other, name="value_grads",
    )
    write_own, value_grad = lax.optimization_barrier((write_own, value_grad))
    pieces = []
    for shift in range(chips):
        piece = value_grad
        if shift:
            piece = lax.ppermute(
                value_grad, "dp", [(i, (i + 2 * shift) % row_devices) for i in range(row_devices)]
            )
        swapped = lax.ppermute(piece, "dp", [(i, i ^ 1) for i in range(row_devices)])
        pieces += [piece, swapped]
    write_other = around(write_own)
    (partial,) = call(
        functools.partial(weight_kernel, row_devices=row_devices),
        [((seq_devices, rows, columns), BF)],
        place, input_rows, *pieces, name="weight_part",
    )
    shares = lax.all_to_all(partial, "sp", 0, 0, tiled=True)
    (token_rows,) = call(
        functools.partial(inputs_kernel, row_devices=row_devices),
        [((row_devices, tokens, rows), BF)],
        place, value_weight, *pieces, name="input_rows",
    )
    grad_inputs = (
        lax.all_to_all(token_rows, "dp", 0, 0, tiled=True)
        .transpose(1, 0, 2)
        .reshape(1, tokens, row_devices * rows)
    )
    grad_queries, grad_keys, grad_decay = call(
        functools.partial(rest_kernel, **sizes),
        [((tokens, width), BF)] * 3,
        place, query, key, value, gate, upstream, before, after, *read_other, *write_other,
        name="other_grads",
    )
    share = jnp.sum(shares.astype(F32), axis=0).astype(BF)
    grad_weight = lax.all_gather(share, "sp", axis=1, tiled=True).astype(F32)
    return (grad_queries[None], grad_keys[None], grad_decay[None], grad_inputs, grad_weight)


def solution(mesh):
    return jax.shard_map(
        per_device,
        mesh=mesh,
        in_specs=(P("dp", "sp", None),) * 6 + (P("dp", None),),
        out_specs=(P("dp", "sp", None),) * 4 + (P("dp", None),),
        check_vma=False,
    )
```

profile of v0, /device:TPU:0, one launch (start us, length us, event | category | flops | bytes accessed | tf_op | source)
XLA Modules:
  0.0 114.2 jit_solution(4338138586238574244)
XLA Ops:
  1.2 2.9 %read_states.1 = (bf16[528,128]{1,0:T(8,128)(2,1)}, bf16[528,128]{1,0:T(8,128)(2,1)}, bf16[528,128]{1,0:T(8,128)(2,1)}) custom-call(s32[2]{0:T(128)} %pad_add_fusion.place, bf16[128,1024]{1,0:T(8,128)(2,1)} %bitcast.19, bf16[128,1024]{1,0:T(8,128)(2,1)} %bitcast.15, bf16[128,1024]{1,0:T(8,128)(2,1)} %bitcast.25), custom_call_target="tpu_custom_call" | custom-call | tf_op jit(solution)/shard_map/read_states/pallas_call | solution.py:290
  4.1 3.1 %collective-permute-start = (bf16[528,128]{1,0:T(8,128)(2,1)}, bf16[528,128]{1,0:T(8,128)(2,1)S(1)}, u32[]{:S(2)}, u32[]{:S(2)}) collective-permute-start(bf16[528,128]{1,0:T(8,128)(2,1)} %get-tuple-element.23), channel_id=1, source_target_pairs={{0,8},{8,16},{16,24},{24,0},{1,9},{9,17},{17,25},{25,1},{2,10},{10... | collective-permute-start | bytes 405512 | tf_op jit(solution)/shard_map/ppermute | solution.py:316
  7.2 2.6 %collective-permute-start.1 = (bf16[528,128]{1,0:T(8,128)(2,1)}, bf16[528,128]{1,0:T(8,128)(2,1)S(1)}, u32[]{:S(2)}, u32[]{:S(2)}) collective-permute-start(bf16[528,128]{1,0:T(8,128)(2,1)} %get-tuple-element.24), channel_id=1, source_target_pairs={{0,16},{8,24},{16,0},{24,8},{1,17},{9,25},{17,1},{25,9},{2,18},{10... | collective-permute-start | bytes 405512 | tf_op jit(solution)/shard_map/ppermute | solution.py:316
  9.7 1.3 %collective-permute-start.2 = (bf16[528,128]{1,0:T(8,128)(2,1)}, bf16[528,128]{1,0:T(8,128)(2,1)S(1)}, u32[]{:S(2)}, u32[]{:S(2)}) collective-permute-start(bf16[528,128]{1,0:T(8,128)(2,1)} %get-tuple-element.25), channel_id=1, source_target_pairs={{0,24},{8,0},{16,8},{24,16},{1,25},{9,1},{17,9},{25,17},{2,26},{10... | collective-permute-start | bytes 405512 | tf_op jit(solution)/shard_map/ppermute | solution.py:316
  11.1 5.3 %inner_values.1 = (f32[128,1024]{1,0:T(8,128)}, bf16[512,128]{1,0:T(8,128)(2,1)}, bf16[512,128]{1,0:T(8,128)(2,1)}, bf16[512,128]{1,0:T(8,128)(2,1)}) custom-call(s32[2]{0:T(128)} %pad_add_fusion.place, bf16[128,1024]{1,0:T(8,128)(2,1)} %bitcast.20, bf16[128,1024]{1,0:T(8,128)(2,1)} %bitcast.22, bf16[128,1024]{1,0:T(8,128)(2,1)} %bitcast.30, ...), custom_call_target="tpu_custom_call" | custom-call | tf_op jit(solution)/shard_map/inner_values/pallas_call | solution.py:290
  16.4 2.4 %collective-permute-done.1.rest_1_ = bf16[528,128]{1,0:T(8,128)(2,1)S(1)} collective-permute-done((bf16[528,128]{1,0:T(8,128)(2,1)}, bf16[528,128]{1,0:T(8,128)(2,1)S(1)}, u32[]{:S(2)}, u32[]{:S(2)}) %collective-permute-start.1) | collective-permute-done | bytes 135200 | tf_op jit(solution)/shard_map/ppermute | solution.py:316
  18.9 0.6 copy-done.10
  19.6 3.0 %value_grads.1 = (bf16[4,128,256]{2,1,0:T(8,128)(2,1)}, f32[512,128]{1,0:T(8,128)}, f32[512,128]{1,0:T(8,128)}) custom-call(s32[2]{0:T(128)} %pad_add_fusion.place, bf16[128,1024]{1,0:T(8,128)(2,1)} %bitcast.23, bf16[128,1024]{1,0:T(8,128)(2,1)} %bitcast.17, f32[128,1024]{1,0:T(8,128)} %get-tuple-element.22.inner_ref, bf16[528,128]{1,0:T(8,128)(2,1)} %copy-done.9, ...), custom_call_target="tpu_custom_call" | custom-call | tf_op jit(solution)/shard_map/value_grads/pallas_call | solution.py:290
  22.5 2.4 %collective-permute-start.11 = (bf16[4,128,256]{2,1,0:T(8,128)(2,1)}, bf16[4,128,256]{2,1,0:T(8,128)(2,1)S(1)}, u32[]{:S(2)}, u32[]{:S(2)}) collective-permute-start(bf16[4,128,256]{2,1,0:T(8,128)(2,1)} %get-tuple-element.38.rest_0_), channel_id=1, source_target_pairs={{0,6},{1,7},{2,0},{3,1},{4,2},{5,3},{6,4},{7,5},{8,14},{9,15},{10,... | collective-permute-start | bytes 786440 | tf_op jit(solution)/shard_map/ppermute | solution.py:346
  25.5 0.6 collective-permute-start.7
  26.1 1.0 copy.14
  27.1 3.8 %all-to-all-start.1 = ((bf16[8,256,128]{2,1,0:T(8,128)(2,1)}), bf16[8,256,128]{2,1,0:T(8,128)(2,1)S(1)}, u32[]{:S(2)}, u32[]{:S(2)}) async-start(bf16[8,256,128]{2,1,0:T(8,128)(2,1)} %bitcast.13), calls=%async_computation.1 | async-start | bytes 1048576 | tf_op jit(solution)/shard_map/all_to_all | solution.py:333
  31.4 0.6 collective-permute-done.11.rest_6_
  32.0 9.7 %collective-permute-done.9.rest_4_ = bf16[4,128,256]{2,1,0:T(8,128)(2,1)S(1)} collective-permute-done((bf16[4,128,256]{2,1,0:T(8,128)(2,1)}, bf16[4,128,256]{2,1,0:T(8,128)(2,1)S(1)}, u32[]{:S(2)}, u32[]{:S(2)}) %collective-permute-start.9) | collective-permute-done | bytes 262176 | tf_op jit(solution)/shard_map/ppermute | solution.py:346
  42.2 1.0 collective-permute-done.10.rest_5_
  43.9 0.7 copy-done.8
  44.6 3.9 %input_rows.1 = bf16[8,128,256]{2,1,0:T(8,128)(2,1)} custom-call(s32[2]{0:T(128)} %pad_add_fusion.place, bf16[256,1024]{1,0:T(8,128)(2,1)} %w_ref.1, bf16[4,128,256]{2,1,0:T(8,128)(2,1)} %get-tuple-element.38.rest_0_, bf16[4,128,256]{2,1,0:T(8,128)(2,1)} %copy-done.5, bf16[4,128,256]{2,1,0:T(8,128)(2,1)} %copy-done.4, bf16[4,128,256]{2,1,0:T(8,128)(2,1)} %copy-done.8, ...), custom_call_target="tpu_custom_call" | custom-call | tf_op jit(solution)/shard_map/input_rows/pallas_call | solution.py:290
  48.5 0.8 copy-done
  49.3 3.5 %all-to-all-start = ((bf16[8,128,256]{2,1,0:T(8,128)(2,1)}), bf16[8,128,256]{2,1,0:T(8,128)(2,1)S(1)}, u32[]{:S(2)}, u32[]{:S(2)}) async-start(bf16[8,128,256]{2,1,0:T(8,128)(2,1)} %input_rows.1), calls=%async_computation | async-start | bytes 1048576 | tf_op jit(solution)/shard_map/all_to_all | solution.py:364
  52.8 3.7 %weight_part.1 = bf16[4,256,256]{2,1,0:T(8,128)(2,1)} custom-call(s32[2]{0:T(128)} %pad_add_fusion.place, bf16[8,256,128]{2,1,0:T(8,128)(2,1)} %copy-done, bf16[4,128,256]{2,1,0:T(8,128)(2,1)} %get-tuple-element.38.rest_0_, bf16[4,128,256]{2,1,0:T(8,128)(2,1)} %copy-done.5, bf16[4,128,256]{2,1,0:T(8,128)(2,1)} %copy-done.4, bf16[4,128,256]{2,1,0:T(8,128)(2,1)} %copy-done.8, ...), custom_call_target="tpu_custom_call" | custom-call | tf_op jit(solution)/shard_map/weight_part/pallas_call | solution.py:290
  56.5 6.0 %all-to-all-done = bf16[8,128,256]{2,1,0:T(8,128)(2,1)S(1)} async-done(((bf16[8,128,256]{2,1,0:T(8,128)(2,1)}), bf16[8,128,256]{2,1,0:T(8,128)(2,1)S(1)}, u32[]{:S(2)}, u32[]{:S(2)}) %all-to-all-start) | async-done | bytes 524320 | tf_op jit(solution)/shard_map/all_to_all | solution.py:364
  62.5 5.0 %all-to-all-start.2 = ((bf16[4,256,256]{2,1,0:T(8,128)(2,1)}), bf16[4,256,256]{2,1,0:T(8,128)(2,1)S(1)}, u32[]{:S(2)}, u32[]{:S(2)}) async-start(bf16[4,256,256]{2,1,0:T(8,128)(2,1)} %weight_part.1), calls=%async_computation.2 | async-start | bytes 1048576 | tf_op jit(solution)/shard_map/all_to_all | solution.py:357
  67.4 2.0 %collective-permute-start.3 = (bf16[512,128]{1,0:T(8,128)(2,1)S(1)}, bf16[512,128]{1,0:T(8,128)(2,1)S(1)}, u32[]{:S(2)}, u32[]{:S(2)}) collective-permute-start(bf16[512,128]{1,0:T(8,128)(2,1)S(1)} %copy-done.18), channel_id=1, source_target_pairs={{0,8},{8,16},{16,24},{24,0},{1,9},{9,17},{17,25},{25,1},{2,10},{10... | collective-permute-start | bytes 393224 | tf_op jit(solution)/shard_map/ppermute | solution.py:316
  69.5 2.4 %collective-permute-start.4 = (bf16[512,128]{1,0:T(8,128)(2,1)S(1)}, bf16[512,128]{1,0:T(8,128)(2,1)S(1)}, u32[]{:S(2)}, u32[]{:S(2)}) collective-permute-start(bf16[512,128]{1,0:T(8,128)(2,1)S(1)} %copy-done.17), channel_id=1, source_target_pairs={{0,16},{8,24},{16,0},{24,8},{1,17},{9,25},{17,1},{25,9},{2,18},{10... | collective-permute-start | bytes 393224 | tf_op jit(solution)/shard_map/ppermute | solution.py:316
  71.8 1.5 %collective-permute-start.5 = (bf16[512,128]{1,0:T(8,128)(2,1)S(1)}, bf16[512,128]{1,0:T(8,128)(2,1)S(1)}, u32[]{:S(2)}, u32[]{:S(2)}) collective-permute-start(bf16[512,128]{1,0:T(8,128)(2,1)S(1)} %copy-done.16), channel_id=1, source_target_pairs={{0,24},{8,0},{16,8},{24,16},{1,25},{9,1},{17,9},{25,17},{2,26},{10... | collective-permute-start | bytes 393224 | tf_op jit(solution)/shard_map/ppermute | solution.py:316
  73.3 10.2 %collective-permute-done.3.rest_3_ = bf16[512,128]{1,0:T(8,128)(2,1)S(1)} collective-permute-done((bf16[512,128]{1,0:T(8,128)(2,1)S(1)}, bf16[512,128]{1,0:T(8,128)(2,1)S(1)}, u32[]{:S(2)}, u32[]{:S(2)}) %collective-permute-start.3) | collective-permute-done | bytes 131104 | tf_op jit(solution)/shard_map/ppermute | solution.py:316
  83.5 6.1 %collective-permute-done.4.rest_4_ = bf16[512,128]{1,0:T(8,128)(2,1)S(1)} collective-permute-done((bf16[512,128]{1,0:T(8,128)(2,1)S(1)}, bf16[512,128]{1,0:T(8,128)(2,1)S(1)}, u32[]{:S(2)}, u32[]{:S(2)}) %collective-permute-start.4) | collective-permute-done | bytes 131104 | tf_op jit(solution)/shard_map/ppermute | solution.py:316
  89.6 0.6 copy-done.14
  90.2 6.6 %other_grads.1 = (bf16[128,1024]{1,0:T(8,128)(2,1)}, bf16[128,1024]{1,0:T(8,128)(2,1)}, bf16[128,1024]{1,0:T(8,128)(2,1)}) custom-call(s32[2]{0:T(128)} %pad_add_fusion.place, bf16[128,1024]{1,0:T(8,128)(2,1)} %bitcast.21, bf16[128,1024]{1,0:T(8,128)(2,1)} %bitcast.24, bf16[128,1024]{1,0:T(8,128)(2,1)} %bitcast.31, bf16[128,1024]{1,0:T(8,128)(2,1)} %bitcast.18, ...), custom_call_target="tpu_custom_call" | custom-call | tf_op jit(solution)/shard_map/other_grads/pallas_call | solution.py:290
  97.1 1.0 copy.15
  98.2 14.9 %all_gather.3 = bf16[256,1024]{1,0:T(8,128)(2,1)S(1)} all-gather(bf16[256,256]{1,0:T(8,128)(2,1)S(1)} %reduce_sum.12), channel_id=1, replica_groups=mesh['sp'=4,'dp'=8] {'sp'}, dimensions={1}, use_global_device_ids=true | all-gather | bytes 655360 | tf_op jit(solution)/shard_map/all_gather | solution.py:375
  113.2 1.1 convert_element_type.2
  (51 shorter events, 3.3 us)
Async XLA Ops:
  4.1 12.3 %collective-permute-start = (bf16[528,128]{1,0:T(8,128)(2,1)}, bf16[528,128]{1,0:T(8,128)(2,1)S(1)}, u32[]{:S(2)}, u32[]{:S(2)}) collective-permute-start(bf16[528,128]{1,0:T(8,128)(2,1)} %get-tuple-element.23), channel_id=1, source_target_pairs={{0,8},{8,16},{16,24},{24,0},{1,9},{9,17},{17,25},{25,1},{2,10},{10... | collective-permute-start | bytes 405512 | tf_op jit(solution)/shard_map/ppermute | solution.py:316
  7.2 11.7 %collective-permute-start.1 = (bf16[528,128]{1,0:T(8,128)(2,1)}, bf16[528,128]{1,0:T(8,128)(2,1)S(1)}, u32[]{:S(2)}, u32[]{:S(2)}) collective-permute-start(bf16[528,128]{1,0:T(8,128)(2,1)} %get-tuple-element.24), channel_id=1, source_target_pairs={{0,16},{8,24},{16,0},{24,8},{1,17},{9,25},{17,1},{25,9},{2,18},{10... | collective-permute-start | bytes 405512 | tf_op jit(solution)/shard_map/ppermute | solution.py:316
  9.7 9.1 %collective-permute-start.2 = (bf16[528,128]{1,0:T(8,128)(2,1)}, bf16[528,128]{1,0:T(8,128)(2,1)S(1)}, u32[]{:S(2)}, u32[]{:S(2)}) collective-permute-start(bf16[528,128]{1,0:T(8,128)(2,1)} %get-tuple-element.25), channel_id=1, source_target_pairs={{0,24},{8,0},{16,8},{24,16},{1,25},{9,1},{17,9},{25,17},{2,26},{10... | collective-permute-start | bytes 405512 | tf_op jit(solution)/shard_map/ppermute | solution.py:316
  16.4 2.4 %copy-start.9 = (bf16[528,128]{1,0:T(8,128)(2,1)}, bf16[528,128]{1,0:T(8,128)(2,1)S(1)}, u32[]{:S(2)}) copy-start(bf16[528,128]{1,0:T(8,128)(2,1)S(1)} %collective-permute-done.rest_0_) | copy-start | bytes 405508
  18.9 0.7 copy-start.11
  19.6 6.5 %copy-start.12 = (bf16[1,128,2048]{2,1,0:T(8,128)(2,1)S(1)}, bf16[1,128,2048]{2,1,0:T(8,128)(2,1)}, u32[]{:S(2)}) copy-start(bf16[1,128,2048]{2,1,0:T(8,128)(2,1)} %param.7) | copy-start | bytes 1572868
  22.5 9.5 %collective-permute-start.11 = (bf16[4,128,256]{2,1,0:T(8,128)(2,1)}, bf16[4,128,256]{2,1,0:T(8,128)(2,1)S(1)}, u32[]{:S(2)}, u32[]{:S(2)}) collective-permute-start(bf16[4,128,256]{2,1,0:T(8,128)(2,1)} %get-tuple-element.38.rest_0_), channel_id=1, source_target_pairs={{0,6},{1,7},{2,0},{3,1},{4,2},{5,3},{6,4},{7,5},{8,14},{9,15},{10,... | collective-permute-start | bytes 786440 | tf_op jit(solution)/shard_map/ppermute | solution.py:346
  25.0 16.7 %collective-permute-start.9 = (bf16[4,128,256]{2,1,0:T(8,128)(2,1)}, bf16[4,128,256]{2,1,0:T(8,128)(2,1)S(1)}, u32[]{:S(2)}, u32[]{:S(2)}) collective-permute-start(bf16[4,128,256]{2,1,0:T(8,128)(2,1)} %get-tuple-element.38.rest_0_), channel_id=1, source_target_pairs={{0,4},{1,5},{2,6},{3,7},{4,0},{5,1},{6,2},{7,3},{8,12},{9,13},{10,... | collective-permute-start | bytes 786440 | tf_op jit(solution)/shard_map/ppermute | solution.py:346
  25.5 16.2 %collective-permute-start.7 = (bf16[4,128,256]{2,1,0:T(8,128)(2,1)}, bf16[4,128,256]{2,1,0:T(8,128)(2,1)S(1)}, u32[]{:S(2)}, u32[]{:S(2)}) collective-permute-start(bf16[4,128,256]{2,1,0:T(8,128)(2,1)} %get-tuple-element.38.rest_0_), channel_id=1, source_target_pairs={{0,2},{1,3},{2,4},{3,5},{4,6},{5,7},{6,0},{7,1},{8,10},{9,11},{10,... | collective-permute-start | bytes 786440 | tf_op jit(solution)/shard_map/ppermute | solution.py:346
  27.1 3.8 %copy-start.1 = (bf16[4,128,256]{2,1,0:T(8,128)(2,1)S(1)}, bf16[4,128,256]{2,1,0:T(8,128)(2,1)}, u32[]{:S(2)}) copy-start(bf16[4,128,256]{2,1,0:T(8,128)(2,1)} %get-tuple-element.38.rest_0_) | copy-start | bytes 786436
  27.1 21.5 %all-to-all-start.1 = ((bf16[8,256,128]{2,1,0:T(8,128)(2,1)}), bf16[8,256,128]{2,1,0:T(8,128)(2,1)S(1)}, u32[]{:S(2)}, u32[]{:S(2)}) async-start(bf16[8,256,128]{2,1,0:T(8,128)(2,1)} %bitcast.13), calls=%async_computation.1 | async-start | bytes 1048576 | tf_op jit(solution)/shard_map/all_to_all | solution.py:333
  30.9 11.3 %collective-permute-start.6 = (bf16[4,128,256]{2,1,0:T(8,128)(2,1)S(1)}, bf16[4,128,256]{2,1,0:T(8,128)(2,1)S(1)}, u32[]{:S(2)}, u32[]{:S(2)}) collective-permute-start(bf16[4,128,256]{2,1,0:T(8,128)(2,1)S(1)} %copy-done.1), channel_id=1, source_target_pairs={{0,1},{1,0},{2,3},{3,2},{4,5},{5,4},{6,7},{7,6},{8,9},{9,8},{10,11... | collective-permute-start | bytes 786440 | tf_op jit(solution)/shard_map/ppermute | solution.py:349
  32.0 11.6 %copy-start.2 = (bf16[4,128,256]{2,1,0:T(8,128)(2,1)}, bf16[4,128,256]{2,1,0:T(8,128)(2,1)S(1)}, u32[]{:S(2)}) copy-start(bf16[4,128,256]{2,1,0:T(8,128)(2,1)S(1)} %collective-permute-done.11.rest_6_) | copy-start | bytes 786436
  32.0 10.2 %collective-permute-start.12 = (bf16[4,128,256]{2,1,0:T(8,128)(2,1)S(1)}, bf16[4,128,256]{2,1,0:T(8,128)(2,1)S(1)}, u32[]{:S(2)}, u32[]{:S(2)}) collective-permute-start(bf16[4,128,256]{2,1,0:T(8,128)(2,1)S(1)} %collective-permute-done.11.rest_6_), channel_id=1, source_target_pairs={{0,1},{1,0},{2,3},{3,2},{4,5},{5,4},{6,7},{7,6},{8,9},{9,8},{10,11... | collective-permute-start | bytes 786440 | tf_op jit(solution)/shard_map/ppermute | solution.py:349
  41.7 1.9 %copy-start.3 = (bf16[4,128,256]{2,1,0:T(8,128)(2,1)}, bf16[4,128,256]{2,1,0:T(8,128)(2,1)S(1)}, u32[]{:S(2)}) copy-start(bf16[4,128,256]{2,1,0:T(8,128)(2,1)S(1)} %collective-permute-done.9.rest_4_) | copy-start | bytes 786436
  41.7 1.5 %collective-permute-start.10 = (bf16[4,128,256]{2,1,0:T(8,128)(2,1)S(1)}, bf16[4,128,256]{2,1,0:T(8,128)(2,1)S(1)}, u32[]{:S(2)}, u32[]{:S(2)}) collective-permute-start(bf16[4,128,256]{2,1,0:T(8,128)(2,1)S(1)} %collective-permute-done.9.rest_4_), channel_id=1, source_target_pairs={{0,1},{1,0},{2,3},{3,2},{4,5},{5,4},{6,7},{7,6},{8,9},{9,8},{10,11... | collective-permute-start | bytes 786440 | tf_op jit(solution)/shard_map/ppermute | solution.py:349
  41.7 1.9 %copy-start.4 = (bf16[4,128,256]{2,1,0:T(8,128)(2,1)}, bf16[4,128,256]{2,1,0:T(8,128)(2,1)S(1)}, u32[]{:S(2)}) copy-start(bf16[4,128,256]{2,1,0:T(8,128)(2,1)S(1)} %collective-permute-done.7.rest_2_) | copy-start | bytes 786436
  41.7 1.9 %collective-permute-start.8 = (bf16[4,128,256]{2,1,0:T(8,128)(2,1)S(1)}, bf16[4,128,256]{2,1,0:T(8,128)(2,1)S(1)}, u32[]{:S(2)}, u32[]{:S(2)}) collective-permute-start(bf16[4,128,256]{2,1,0:T(8,128)(2,1)S(1)} %collective-permute-done.7.rest_2_), channel_id=1, source_target_pairs={{0,1},{1,0},{2,3},{3,2},{4,5},{5,4},{6,7},{7,6},{8,9},{9,8},{10,11... | collective-permute-start | bytes 786440 | tf_op jit(solution)/shard_map/ppermute | solution.py:349
  42.2 1.4 %copy-start.5 = (bf16[4,128,256]{2,1,0:T(8,128)(2,1)}, bf16[4,128,256]{2,1,0:T(8,128)(2,1)S(1)}, u32[]{:S(2)}) copy-start(bf16[4,128,256]{2,1,0:T(8,128)(2,1)S(1)} %collective-permute-done.6.rest_1_) | copy-start | bytes 786436
  42.2 1.4 %copy-start.6 = (bf16[4,128,256]{2,1,0:T(8,128)(2,1)}, bf16[4,128,256]{2,1,0:T(8,128)(2,1)S(1)}, u32[]{:S(2)}) copy-start(bf16[4,128,256]{2,1,0:T(8,128)(2,1)S(1)} %collective-permute-done.12.rest_7_) | copy-start | bytes 786436
  43.2 0.7 copy-start.7
  48.5 0.8 copy-start
  49.3 13.2 %all-to-all-start = ((bf16[8,128,256]{2,1,0:T(8,128)(2,1)}), bf16[8,128,256]{2,1,0:T(8,128)(2,1)S(1)}, u32[]{:S(2)}, u32[]{:S(2)}) async-start(bf16[8,128,256]{2,1,0:T(8,128)(2,1)} %input_rows.1), calls=%async_computation | async-start | bytes 1048576 | tf_op jit(solution)/shard_map/all_to_all | solution.py:364
  56.5 10.9 %copy-start.18 = (bf16[512,128]{1,0:T(8,128)(2,1)S(1)}, bf16[512,128]{1,0:T(8,128)(2,1)}, u32[]{:S(2)}) copy-start(bf16[512,128]{1,0:T(8,128)(2,1)} %get-tuple-element.32) | copy-start | bytes 393220
  56.5 12.9 %copy-start.17 = (bf16[512,128]{1,0:T(8,128)(2,1)S(1)}, bf16[512,128]{1,0:T(8,128)(2,1)}, u32[]{:S(2)}) copy-start(bf16[512,128]{1,0:T(8,128)(2,1)} %get-tuple-element.33) | copy-start | bytes 393220
  56.5 15.3 %copy-start.16 = (bf16[512,128]{1,0:T(8,128)(2,1)S(1)}, bf16[512,128]{1,0:T(8,128)(2,1)}, u32[]{:S(2)}) copy-start(bf16[512,128]{1,0:T(8,128)(2,1)} %get-tuple-element.34) | copy-start | bytes 393220
  62.5 35.6 %all-to-all-start.2 = ((bf16[4,256,256]{2,1,0:T(8,128)(2,1)}), bf16[4,256,256]{2,1,0:T(8,128)(2,1)S(1)}, u32[]{:S(2)}, u32[]{:S(2)}) async-start(bf16[4,256,256]{2,1,0:T(8,128)(2,1)} %weight_part.1), calls=%async_computation.2 | async-start | bytes 1048576 | tf_op jit(solution)/shard_map/all_to_all | solution.py:357
  67.4 16.0 %collective-permute-start.3 = (bf16[512,128]{1,0:T(8,128)(2,1)S(1)}, bf16[512,128]{1,0:T(8,128)(2,1)S(1)}, u32[]{:S(2)}, u32[]{:S(2)}) collective-permute-start(bf16[512,128]{1,0:T(8,128)(2,1)S(1)} %copy-done.18), channel_id=1, source_target_pairs={{0,8},{8,16},{16,24},{24,0},{1,9},{9,17},{17,25},{25,1},{2,10},{10... | collective-permute-start | bytes 393224 | tf_op jit(solution)/shard_map/ppermute | solution.py:316
  69.5 20.1 %collective-permute-start.4 = (bf16[512,128]{1,0:T(8,128)(2,1)S(1)}, bf16[512,128]{1,0:T(8,128)(2,1)S(1)}, u32[]{:S(2)}, u32[]{:S(2)}) collective-permute-start(bf16[512,128]{1,0:T(8,128)(2,1)S(1)} %copy-done.17), channel_id=1, source_target_pairs={{0,16},{8,24},{16,0},{24,8},{1,17},{9,25},{17,1},{25,9},{2,18},{10... | collective-permute-start | bytes 393224 | tf_op jit(solution)/shard_map/ppermute | solution.py:316
  71.8 17.7 %collective-permute-start.5 = (bf16[512,128]{1,0:T(8,128)(2,1)S(1)}, bf16[512,128]{1,0:T(8,128)(2,1)S(1)}, u32[]{:S(2)}, u32[]{:S(2)}) collective-permute-start(bf16[512,128]{1,0:T(8,128)(2,1)S(1)} %copy-done.16), channel_id=1, source_target_pairs={{0,24},{8,0},{16,8},{24,16},{1,25},{9,1},{17,9},{25,17},{2,26},{10... | collective-permute-start | bytes 393224 | tf_op jit(solution)/shard_map/ppermute | solution.py:316
  83.5 6.1 %copy-start.13 = (bf16[512,128]{1,0:T(8,128)(2,1)}, bf16[512,128]{1,0:T(8,128)(2,1)S(1)}, u32[]{:S(2)}) copy-start(bf16[512,128]{1,0:T(8,128)(2,1)S(1)} %collective-permute-done.3.rest_3_) | copy-start | bytes 393220
  89.6 0.7 copy-start.15
  (3 other events, 2.0 us)
where the time goes:
time: 115 us; the launch traced here: 114 us
  waiting for transfers between devices  36.3 us (32%)
  starting transfers between devices  29.6 us (26%)
  Pallas kernels  25.4 us (22%)
  blocking collectives  14.9 us (13%)
  local copies, waits for them, and re-layouts  5.47 us (5%)
  other arithmetic  1.76 us (2%)
    pallas_call x6, Pallas kernels, call(): pl.pallas_call(body, out_shape=[jax.ShapeDtypeStruct(shape, dtype) for sh...  25.4 us
    ppermute x6, waiting for transfers between devices, around(): lax.ppermute(message, 'sp', [(i, (i + shift) % seq_devices) for i in rang...  18.7 us
    all_gather x1, blocking collectives, per_device(): grad_weight = lax.all_gather(share, 'sp', axis=1, tiled=True).astype(F32)  14.9 us
    ppermute x6, starting transfers between devices, around(): lax.ppermute(message, 'sp', [(i, (i + shift) % seq_devices) for i in rang...  12.8 us
    ppermute x3, waiting for transfers between devices, per_device(): lax.ppermute(value_grad, 'dp', [(i, (i + 2 * shift) % row_devices) for i...  10.3 us
    all_to_all x1, waiting for transfers between devices, per_device(): lax.all_to_all(token_rows, 'dp', 0, 0, tiled=True).transpose(1, 0, 2)  5.95 us
    unnamed x40, local copies, waits for them, and re-layouts  5.2 us
    all_to_all x1, starting transfers between devices, per_device(): shares = lax.all_to_all(partial, 'sp', 0, 0, tiled=True)  4.96 us
  transfers between devices with their start and end apart: 16, of which 8 were waited for; matrix products, arithmetic and copies ran while one was open for 2% of the time, Pallas kernels for 17%

commit v1 on v0

--- a/solution.py
+++ b/solution.py
@@ -158,8 +158,9 @@
 
 def values_kernel(place, k_ref, g_ref, inner_ref, *rest, pairs, seq_devices):
     me = place[0]
-    messages = rest[: seq_devices - 1]
-    value_ref, before_ref, after_ref = rest[seq_devices - 1 :]
+    count = seq_devices - 1
+    messages = rest[:count]
+    value_ref, before_ref, after_ref = rest[2 * count + 1 : 2 * count + 4]
     width = value_ref.shape[2]
     for pair in range(pairs):
         at = lanes(pair)
@@ -190,7 +191,7 @@
     count = seq_devices - 1
     read_messages = rest[:count]
     write_messages = rest[count : 2 * count]
-    gq_ref, gk_ref, gg_ref = rest[2 * count :]
+    gq_ref, gk_ref, gg_ref = rest[-3:]
     length = q_ref.shape[0]
     row, col = iotas(length, length)
     tail = (row <= col).astype(BF)
@@ -262,19 +263,20 @@
     return 2 * chip + (core if step % 2 == 0 else 1 - core)
 
 
-def weight_kernel(place, x_ref, *rest, row_devices):
+def weight_kernel(place, x_ref, *rest, row_devices, seq_devices):
     pieces = rest[:row_devices]
-    out_ref = rest[row_devices]
-    for block in range(out_ref.shape[0]):
-        acc = jnp.zeros(out_ref.shape[1:], F32)
+    outs = rest[-seq_devices:]
+    for shift, out_ref in enumerate(outs):
+        block = lax.rem(place[0] + shift, seq_devices)
+        acc = jnp.zeros(out_ref.shape, F32)
         for step in range(row_devices):
             acc = acc + dot(x_ref[source_of(place, step, row_devices)], pieces[step][block], 1, 0)
-        out_ref[block] = acc.astype(BF)
+        out_ref[...] = acc.astype(out_ref.dtype)
 
 
 def inputs_kernel(place, w_ref, *rest, row_devices):
     pieces = rest[:row_devices]
-    out_ref = rest[row_devices]
+    out_ref = rest[-1]
     blocks, _, width = pieces[0].shape
     for step in range(row_devices):
         acc = jnp.zeros(out_ref.shape[1:], F32)
@@ -283,17 +285,33 @@
         out_ref[source_of(place, step, row_devices)] = acc.astype(BF)
 
 
-def call(body, shapes, place, *operands, name):
-    specs = [pl.BlockSpec(memory_space=pltpu.SMEM)] + [
-        pl.BlockSpec(memory_space=pltpu.VMEM) for _ in operands
-    ]
+def join_kernel(place, *rest, seq_devices):
+    out_ref = rest[-1]
+    width = rest[0].shape[1]
+    for shift in range(seq_devices):
+        source = lax.rem(place[0] + seq_devices - shift, seq_devices)
+        for block in range(seq_devices):
+
+            @pl.when(source == block)
+            def _(shift=shift, block=block):
+                out_ref[:, block * width : (block + 1) * width] = rest[shift][...].astype(F32)
+
+
+def call(body, shapes, place, *operands, name, waits=(), through=()):
+    vmem = pl.BlockSpec(memory_space=pltpu.VMEM)
+    anywhere = pl.BlockSpec(memory_space=pl.ANY)
+    first = 1 + len(operands) + len(waits)
     return pl.pallas_call(
         body,
-        out_shape=[jax.ShapeDtypeStruct(shape, dtype) for shape, dtype in shapes],
-        in_specs=specs,
-        out_specs=[pl.BlockSpec(memory_space=pltpu.VMEM) for _ in shapes],
+        out_shape=[jax.ShapeDtypeStruct(shape, dtype) for shape, dtype in shapes]
+        + [jax.ShapeDtypeStruct(array.shape, array.dtype) for array in through],
+        in_specs=[pl.BlockSpec(memory_space=pltpu.SMEM)]
+        + [vmem] * len(operands)
+        + [anywhere] * (len(waits) + len(through)),
+        out_specs=[vmem] * len(shapes) + [anywhere] * len(through),
+        input_output_aliases={first + i: len(shapes) + i for i in range(len(through))},
         name=name,
-    )(place, *operands)
+    )(place, *operands, *waits, *through)
 
 
 def per_device(inputs, queries, keys, values, log_decay, cotangent, value_weight):
@@ -333,12 +351,12 @@
     input_rows = lax.all_to_all(
         inputs[0].reshape(tokens, row_devices, rows).transpose(1, 2, 0), "dp", 0, 0, tiled=True
     )
-    value_grad, before, after = call(
+    value_grad, before, after, *write_own = call(
         functools.partial(values_kernel, **sizes),
         [((seq_devices, tokens, columns), BF)] + [((pairs * HEAD_DIM, PAIR), F32)] * 2,
         place, key, gate, inner, *read_other, name="value_grads",
-    )
-    write_own, value_grad = lax.optimization_barrier((write_own, value_grad))
+        waits=(input_rows,), through=write_own,
+    )
     pieces = []
     for shift in range(chips):
         piece = value_grad
@@ -349,16 +367,16 @@
         swapped = lax.ppermute(piece, "dp", [(i, i ^ 1) for i in range(row_devices)])
         pieces += [piece, swapped]
     write_other = around(write_own)
-    (partial,) = call(
-        functools.partial(weight_kernel, row_devices=row_devices),
-        [((seq_devices, rows, columns), BF)],
-        place, input_rows, *pieces, name="weight_part",
-    )
-    shares = lax.all_to_all(partial, "sp", 0, 0, tiled=True)
+    partial = call(
+        functools.partial(weight_kernel, row_devices=row_devices, seq_devices=seq_devices),
+        [((rows, columns), F32)] + [((rows, columns), BF)] * count,
+        place, input_rows, *pieces, name="weight_part", waits=write_other,
+    )
+    shares = around(partial[1:])
     (token_rows,) = call(
         functools.partial(inputs_kernel, row_devices=row_devices),
         [((row_devices, tokens, rows), BF)],
-        place, value_weight, *pieces, name="input_rows",
+        place, value_weight, *pieces, name="input_rows", waits=partial[:1],
     )
     grad_inputs = (
         lax.all_to_all(token_rows, "dp", 0, 0, tiled=True)
@@ -369,10 +387,14 @@
         functools.partial(rest_kernel, **sizes),
         [((tokens, width), BF)] * 3,
         place, query, key, value, gate, upstream, before, after, *read_other, *write_other,
-        name="other_grads",
-    )
-    share = jnp.sum(shares.astype(F32), axis=0).astype(BF)
-    grad_weight = lax.all_gather(share, "sp", axis=1, tiled=True).astype(F32)
+        name="other_grads", waits=(token_rows,),
+    )
+    share = (partial[0] + sum(part.astype(F32) for part in shares)).astype(BF)
+    (grad_weight,) = call(
+        functools.partial(join_kernel, seq_devices=seq_devices),
+        [((rows, width), F32)],
+        place, share, *around([share] * count), name="join",
+    )
     return (grad_queries[None], grad_keys[None], grad_decay[None], grad_inputs, grad_weight)
 
 

time: 115 us -> 93.1 us (0.81)
  waiting for transfers between devices: 36.3 us -> 19.7 us
  blocking collectives: 14.9 us -> 0 us
  starting transfers between devices: 29.6 us -> 37 us
  Pallas kernels: 25.4 us -> 27.5 us
  local copies, waits for them, and re-layouts: 5.47 us -> 7.06 us
    all_gather x1 -> x0, blocking collectives: 14.9 us -> none  [per_device(): grad_weight = lax.all_gather(share, 'sp', axis=1, tiled=True).astype(F32)]
    ppermute x6 -> x12, starting transfers between devices: 12.8 us -> 23.5 us  [around(): lax.ppermute(message, 'sp', [(i, (i + shift) % seq_devices) for i in rang...]
    ppermute x3, waiting for transfers between devices: 10.3 us -> 3.49 us  [per_device(): lax.ppermute(value_grad, 'dp', [(i, (i + 2 * shift) % row_devices) for i...]
    all_to_all x1, waiting for transfers between devices: 5.95 us -> 0.01 us  [per_device(): lax.all_to_all(token_rows, 'dp', 0, 0, tiled=True).transpose(1, 0, 2)]
    all_to_all x1 -> x0, starting transfers between devices: 4.96 us -> none  [per_device(): shares = lax.all_to_all(partial, 'sp', 0, 0, tiled=True)]
    ppermute x6 -> x12, waiting for transfers between devices: 18.7 us -> 16.2 us  [around(): lax.ppermute(message, 'sp', [(i, (i + shift) % seq_devices) for i in rang...]
    pallas_call x6 -> x7, Pallas kernels: 25.4 us -> 27.5 us  [call(): pl.pallas_call(body, out_shape=[jax.ShapeDtypeStruct(shape, dtype) for sh...]
    unnamed x40, local copies, waits for them, and re-layouts: 5.2 us -> 6.79 us
  transfers between devices with their start and end apart: 16 -> 21, of which waited for: 8 -> 7; matrix products, arithmetic and copies ran while one was open for 2% -> 1% of each run, Pallas kernels for 17% -> 23%
where the time goes in v1:
time: 93.1 us; the launch traced here: 92.6 us
  starting transfers between devices  37 us (40%)
  Pallas kernels  27.5 us (30%)
  waiting for transfers between devices  19.7 us (21%)
  local copies, waits for them, and re-layouts  7.06 us (8%)
    pallas_call x7, Pallas kernels, call(): pl.pallas_call(body, out_shape=[jax.ShapeDtypeStruct(shape, dtype) for sh...  27.5 us
    ppermute x12, starting transfers between devices, around(): lax.ppermute(message, 'sp', [(i, (i + shift) % seq_devices) for i in rang...  23.5 us
    ppermute x12, waiting for transfers between devices, around(): lax.ppermute(message, 'sp', [(i, (i + shift) % seq_devices) for i in rang...  16.2 us
    unnamed x40, local copies, waits for them, and re-layouts  6.79 us
    all_to_all x1, starting transfers between devices, per_device(): lax.all_to_all(inputs[0].reshape(tokens, row_devices, rows).transpose(1,...  5.2 us
    ppermute x3, starting transfers between devices, per_device(): lax.ppermute(value_grad, 'dp', [(i, (i + 2 * shift) % row_devices) for i...  3.69 us
    all_to_all x1, starting transfers between devices, per_device(): lax.all_to_all(token_rows, 'dp', 0, 0, tiled=True).transpose(1, 0, 2)  3.63 us
    ppermute x3, waiting for transfers between devices, per_device(): lax.ppermute(value_grad, 'dp', [(i, (i + 2 * shift) % row_devices) for i...  3.49 us
  transfers between devices with their start and end apart: 21, of which 7 were waited for; matrix products, arithmetic and copies ran while one was open for 1% of the time, Pallas kernels for 23%

profile of v1, /device:TPU:0, one launch (start us, length us, event | category | flops | bytes accessed | tf_op | source)
XLA Modules:
  0.0 92.6 jit_solution(9178755759016407151)
XLA Ops:
  0.6 2.0 %copy.16 = bf16[1,128,2048]{1,2,0:T(8,128)(2,1)} copy(bf16[1,128,2048]{2,1,0:T(8,128)(2,1)} %param.7) | data formatting | bytes 1048576 | tf_op args[0]
  2.7 5.2 %all-to-all-start = ((bf16[8,256,128]{2,1,0:T(8,128)(2,1)}), bf16[8,256,128]{2,1,0:T(8,128)(2,1)S(1)}, u32[]{:S(2)}, u32[]{:S(2)}) async-start(bf16[8,256,128]{2,1,0:T(8,128)(2,1)} %bitcast.8), calls=%async_computation | async-start | bytes 1048576 | tf_op jit(solution)/shard_map/all_to_all | solution.py:351
  8.4 2.9 %read_states.1 = (bf16[528,128]{1,0:T(8,128)(2,1)}, bf16[528,128]{1,0:T(8,128)(2,1)}, bf16[528,128]{1,0:T(8,128)(2,1)}) custom-call(s32[2]{0:T(128)} %pad_add_fusion.place, bf16[128,1024]{1,0:T(8,128)(2,1)} %bitcast.19, bf16[128,1024]{1,0:T(8,128)(2,1)} %bitcast.15, bf16[128,1024]{1,0:T(8,128)(2,1)} %bitcast.22), custom_call_target="tpu_custom_call" | custom-call | tf_op jit(solution)/shard_map/read_states/pallas_call | solution.py:304
  11.3 1.6 %collective-permute-start = (bf16[528,128]{1,0:T(8,128)(2,1)}, bf16[528,128]{1,0:T(8,128)(2,1)S(1)}, u32[]{:S(2)}, u32[]{:S(2)}) collective-permute-start(bf16[528,128]{1,0:T(8,128)(2,1)} %get-tuple-element.26), channel_id=1, source_target_pairs={{0,8},{8,16},{16,24},{24,0},{1,9},{9,17},{17,25},{25,1},{2,10},{10... | collective-permute-start | bytes 405512 | tf_op jit(solution)/shard_map/ppermute | solution.py:334
  12.9 2.6 %collective-permute-start.1 = (bf16[528,128]{1,0:T(8,128)(2,1)}, bf16[528,128]{1,0:T(8,128)(2,1)S(1)}, u32[]{:S(2)}, u32[]{:S(2)}) collective-permute-start(bf16[528,128]{1,0:T(8,128)(2,1)} %get-tuple-element.27), channel_id=1, source_target_pairs={{0,16},{8,24},{16,0},{24,8},{1,17},{9,25},{17,1},{25,9},{2,18},{10... | collective-permute-start | bytes 405512 | tf_op jit(solution)/shard_map/ppermute | solution.py:334
  15.5 1.3 %collective-permute-start.2 = (bf16[528,128]{1,0:T(8,128)(2,1)}, bf16[528,128]{1,0:T(8,128)(2,1)S(1)}, u32[]{:S(2)}, u32[]{:S(2)}) collective-permute-start(bf16[528,128]{1,0:T(8,128)(2,1)} %get-tuple-element.28), channel_id=1, source_target_pairs={{0,24},{8,0},{16,8},{24,16},{1,25},{9,1},{17,9},{25,17},{2,26},{10... | collective-permute-start | bytes 405512 | tf_op jit(solution)/shard_map/ppermute | solution.py:334
  16.8 5.3 %inner_values.1 = (f32[128,1024]{1,0:T(8,128)}, bf16[512,128]{1,0:T(8,128)(2,1)}, bf16[512,128]{1,0:T(8,128)(2,1)}, bf16[512,128]{1,0:T(8,128)(2,1)}) custom-call(s32[2]{0:T(128)} %pad_add_fusion.place, bf16[128,1024]{1,0:T(8,128)(2,1)} %bitcast.20, bf16[128,1024]{1,0:T(8,128)(2,1)} %bitcast.25, bf16[128,1024]{1,0:T(8,128)(2,1)} %bitcast.30, ...), custom_call_target="tpu_custom_call" | custom-call | tf_op jit(solution)/shard_map/inner_values/pallas_call | solution.py:304
  22.2 3.0 %collective-permute-done.1.rest_1_ = bf16[528,128]{1,0:T(8,128)(2,1)S(1)} collective-permute-done((bf16[528,128]{1,0:T(8,128)(2,1)}, bf16[528,128]{1,0:T(8,128)(2,1)S(1)}, u32[]{:S(2)}, u32[]{:S(2)}) %collective-permute-start.1) | collective-permute-done | bytes 135200 | tf_op jit(solution)/shard_map/ppermute | solution.py:334
  25.3 0.6 copy-done.10
  26.1 2.9 %value_grads.1 = (bf16[4,128,256]{2,1,0:T(8,128)(2,1)}, f32[512,128]{1,0:T(8,128)}, f32[512,128]{1,0:T(8,128)}, bf16[512,128]{1,0:T(8,128)(2,1)}, bf16[512,128]{1,0:T(8,128)(2,1)}, /*index=5*/bf16[512,128]{1,0:T(8,128)(2,1)}) custom-call(s32[2]{0:T(128)} %pad_add_fusion.place, ...), custom_call_target="tpu_custom_call", output_to_operand_aliasing={{3}: (8, {}), {4}: (9, {}), {5}: (10, {})} | custom-call | tf_op jit(solution)/shard_map/value_grads/pallas_call | solution.py:304
  29.0 2.6 %collective-permute-start.11 = (bf16[4,128,256]{2,1,0:T(8,128)(2,1)}, bf16[4,128,256]{2,1,0:T(8,128)(2,1)S(1)}, u32[]{:S(2)}, u32[]{:S(2)}) collective-permute-start(bf16[4,128,256]{2,1,0:T(8,128)(2,1)} %get-tuple-element.37.rest_0_), channel_id=1, source_target_pairs={{0,6},{1,7},{2,0},{3,1},{4,2},{5,3},{6,4},{7,5},{8,14},{9,15},{10,... | collective-permute-start | bytes 786440 | tf_op jit(solution)/shard_map/ppermute | solution.py:364
  32.7 3.3 %collective-permute-start.3 = (bf16[512,128]{1,0:T(8,128)(2,1)}, bf16[512,128]{1,0:T(8,128)(2,1)S(1)}, u32[]{:S(2)}, u32[]{:S(2)}) collective-permute-start(bf16[512,128]{1,0:T(8,128)(2,1)} %get-tuple-element.34), channel_id=1, source_target_pairs={{0,8},{8,16},{16,24},{24,0},{1,9},{9,17},{17,25},{25,1},{2,10},{10... | collective-permute-start | bytes 393224 | tf_op jit(solution)/shard_map/ppermute | solution.py:334
  36.0 1.7 %collective-permute-start.4 = (bf16[512,128]{1,0:T(8,128)(2,1)}, bf16[512,128]{1,0:T(8,128)(2,1)S(1)}, u32[]{:S(2)}, u32[]{:S(2)}) collective-permute-start(bf16[512,128]{1,0:T(8,128)(2,1)} %get-tuple-element.35), channel_id=1, source_target_pairs={{0,16},{8,24},{16,0},{24,8},{1,17},{9,25},{17,1},{25,9},{2,18},{10... | collective-permute-start | bytes 393224 | tf_op jit(solution)/shard_map/ppermute | solution.py:334
  37.7 3.6 %collective-permute-done.3.rest_8_.rest_3_ = bf16[512,128]{1,0:T(8,128)(2,1)S(1)} collective-permute-done((bf16[512,128]{1,0:T(8,128)(2,1)}, bf16[512,128]{1,0:T(8,128)(2,1)S(1)}, u32[]{:S(2)}, u32[]{:S(2)}) %collective-permute-start.3) | collective-permute-done | bytes 131104 | tf_op jit(solution)/shard_map/ppermute | solution.py:334
  41.8 3.5 %collective-permute-done.9.rest_4_ = bf16[4,128,256]{2,1,0:T(8,128)(2,1)S(1)} collective-permute-done((bf16[4,128,256]{2,1,0:T(8,128)(2,1)}, bf16[4,128,256]{2,1,0:T(8,128)(2,1)S(1)}, u32[]{:S(2)}, u32[]{:S(2)}) %collective-permute-start.9) | collective-permute-done | bytes 262176 | tf_op jit(solution)/shard_map/ppermute | solution.py:364
  45.8 3.8 %collective-permute-start.5 = (bf16[512,128]{1,0:T(8,128)(2,1)}, bf16[512,128]{1,0:T(8,128)(2,1)S(1)}, u32[]{:S(2)}, u32[]{:S(2)}) collective-permute-start(bf16[512,128]{1,0:T(8,128)(2,1)} %get-tuple-element.36), channel_id=1, source_target_pairs={{0,24},{8,0},{16,8},{24,16},{1,25},{9,1},{17,9},{25,17},{2,26},{10... | collective-permute-start | bytes 393224 | tf_op jit(solution)/shard_map/ppermute | solution.py:334
  49.6 3.6 %collective-permute-done.5.rest_10_.rest_5_ = bf16[512,128]{1,0:T(8,128)(2,1)S(1)} collective-permute-done((bf16[512,128]{1,0:T(8,128)(2,1)}, bf16[512,128]{1,0:T(8,128)(2,1)S(1)}, u32[]{:S(2)}, u32[]{:S(2)}) %collective-permute-start.5) | collective-permute-done | bytes 131104 | tf_op jit(solution)/shard_map/ppermute | solution.py:334
  54.1 0.7 copy-done.7
  54.8 3.6 %weight_part.1 = (f32[256,256]{1,0:T(8,128)}, bf16[256,256]{1,0:T(8,128)(2,1)}, bf16[256,256]{1,0:T(8,128)(2,1)}, bf16[256,256]{1,0:T(8,128)(2,1)}) custom-call(s32[2]{0:T(128)} %pad_add_fusion.place, bf16[8,256,128]{2,1,0:T(8,128)(2,1)} %copy-done, bf16[4,128,256]{2,1,0:T(8,128)(2,1)} %get-tuple-element.37.rest_0_, bf16[4,128,256]{2,1,0:T(8,128)(2,1)} %copy-done.4, ...), custom_call_target="tpu_custom_call" | custom-call | tf_op jit(solution)/shard_map/weight_part/pallas_call | solution.py:304
  58.4 1.7 %collective-permute-start.13 = (bf16[256,256]{1,0:T(8,128)(2,1)}, bf16[256,256]{1,0:T(8,128)(2,1)S(1)}, u32[]{:S(2)}, u32[]{:S(2)}) collective-permute-start(bf16[256,256]{1,0:T(8,128)(2,1)} %get-tuple-element.42), channel_id=1, source_target_pairs={{0,8},{8,16},{16,24},{24,0},{1,9},{9,17},{17,25},{25,1},{2,10},{10... | collective-permute-start | bytes 393224 | tf_op jit(solution)/shard_map/ppermute | solution.py:334
  60.2 2.7 %collective-permute-start.14 = (bf16[256,256]{1,0:T(8,128)(2,1)}, bf16[256,256]{1,0:T(8,128)(2,1)S(1)}, u32[]{:S(2)}, u32[]{:S(2)}) collective-permute-start(bf16[256,256]{1,0:T(8,128)(2,1)} %get-tuple-element.43), channel_id=1, source_target_pairs={{0,16},{8,24},{16,0},{24,8},{1,17},{9,25},{17,1},{25,9},{2,18},{10... | collective-permute-start | bytes 393224 | tf_op jit(solution)/shard_map/ppermute | solution.py:334
  62.9 3.9 %input_rows.1.rest_6_ = bf16[8,128,256]{2,1,0:T(8,128)(2,1)} custom-call(s32[2]{0:T(128)} %pad_add_fusion.place, bf16[256,1024]{1,0:T(8,128)(2,1)} %w_ref.1, bf16[4,128,256]{2,1,0:T(8,128)(2,1)} %get-tuple-element.37.rest_0_, bf16[4,128,256]{2,1,0:T(8,128)(2,1)} %copy-done.4, bf16[4,128,256]{2,1,0:T(8,128)(2,1)} %copy-done.3, ...), custom_call_target="tpu_custom_call" | custom-call | tf_op jit(solution)/shard_map/input_rows/pallas_call | solution.py:304
  66.8 3.6 %all-to-all-start.1 = ((bf16[8,128,256]{2,1,0:T(8,128)(2,1)}), bf16[8,128,256]{2,1,0:T(8,128)(2,1)S(1)}, u32[]{:S(2)}, u32[]{:S(2)}) async-start(bf16[8,128,256]{2,1,0:T(8,128)(2,1)} %input_rows.1.rest_6_), calls=%async_computation.1 | async-start | bytes 1048576 | tf_op jit(solution)/shard_map/all_to_all | solution.py:382
  70.4 0.7 collective-permute-done.14
  71.2 3.0 %collective-permute-start.18 = (bf16[256,256]{1,0:T(8,128)(2,1)S(1)}, bf16[256,256]{1,0:T(8,128)(2,1)S(1)}, u32[]{:S(2)}, u32[]{:S(2)}) collective-permute-start(bf16[256,256]{1,0:T(8,128)(2,1)S(1)} %add_convert_fusion.rest_0_), channel_id=1, source_target_pairs={{0,24},{8,0},{16,8},{24,16},{1,25},{9,1},{17,9},{25,17},{2,26},{10... | collective-permute-start | bytes 393224 | tf_op jit(solution)/shard_map/ppermute | solution.py:334
  74.2 1.7 %collective-permute-start.17 = (bf16[256,256]{1,0:T(8,128)(2,1)S(1)}, bf16[256,256]{1,0:T(8,128)(2,1)S(1)}, u32[]{:S(2)}, u32[]{:S(2)}) collective-permute-start(bf16[256,256]{1,0:T(8,128)(2,1)S(1)} %add_convert_fusion.rest_0_), channel_id=1, source_target_pairs={{0,16},{8,24},{16,0},{24,8},{1,17},{9,25},{17,1},{25,9},{2,18},{10... | collective-permute-start | bytes 393224 | tf_op jit(solution)/shard_map/ppermute | solution.py:334
  76.0 6.6 %other_grads.1 = (bf16[128,1024]{1,0:T(8,128)(2,1)}, bf16[128,1024]{1,0:T(8,128)(2,1)}, bf16[128,1024]{1,0:T(8,128)(2,1)}) custom-call(s32[2]{0:T(128)} %pad_add_fusion.place, bf16[128,1024]{1,0:T(8,128)(2,1)} %bitcast.21, bf16[128,1024]{1,0:T(8,128)(2,1)} %bitcast.27, bf16[128,1024]{1,0:T(8,128)(2,1)} %bitcast.31, bf16[128,1024]{1,0:T(8,128)(2,1)} %bitcast.18, ...), custom_call_target="tpu_custom_call" | custom-call | tf_op jit(solution)/shard_map/other_grads/pallas_call | solution.py:304
  82.6 5.2 %collective-permute-done.17.rest_2_ = bf16[256,256]{1,0:T(8,128)(2,1)S(1)} collective-permute-done((bf16[256,256]{1,0:T(8,128)(2,1)S(1)}, bf16[256,256]{1,0:T(8,128)(2,1)S(1)}, u32[]{:S(2)}, u32[]{:S(2)}) %collective-permute-start.17) | collective-permute-done | bytes 131104 | tf_op jit(solution)/shard_map/ppermute | solution.py:334
  87.8 0.6 copy-done.17
  88.4 0.6 copy-done.18
  89.1 2.2 %join.1 = f32[256,1024]{1,0:T(8,128)} custom-call(s32[2]{0:T(128)} %pad_add_fusion.place, bf16[256,256]{1,0:T(8,128)(2,1)} %copy-done.12, bf16[256,256]{1,0:T(8,128)(2,1)} %copy-done.18, bf16[256,256]{1,0:T(8,128)(2,1)} %copy-done.17, bf16[256,256]{1,0:T(8,128)(2,1)} %copy-done.16), custom_call_target="tpu_custom_call" | custom-call | tf_op jit(solution)/shard_map/join/pallas_call | solution.py:304
  91.6 1.0 %copy.18 = bf16[1,128,2048]{2,1,0:T(8,128)(2,1)} copy(bf16[1,128,2048]{1,2,0:T(8,128)(2,1)S(1)} %bitcast.29) | data formatting | bytes 1048576
  (60 shorter events, 4.2 us)
Async XLA Ops:
  2.7 22.6 %all-to-all-start = ((bf16[8,256,128]{2,1,0:T(8,128)(2,1)}), bf16[8,256,128]{2,1,0:T(8,128)(2,1)S(1)}, u32[]{:S(2)}, u32[]{:S(2)}) async-start(bf16[8,256,128]{2,1,0:T(8,128)(2,1)} %bitcast.8), calls=%async_computation | async-start | bytes 1048576 | tf_op jit(solution)/shard_map/all_to_all | solution.py:351
  11.3 10.9 %collective-permute-start = (bf16[528,128]{1,0:T(8,128)(2,1)}, bf16[528,128]{1,0:T(8,128)(2,1)S(1)}, u32[]{:S(2)}, u32[]{:S(2)}) collective-permute-start(bf16[528,128]{1,0:T(8,128)(2,1)} %get-tuple-element.26), channel_id=1, source_target_pairs={{0,8},{8,16},{16,24},{24,0},{1,9},{9,17},{17,25},{25,1},{2,10},{10... | collective-permute-start | bytes 405512 | tf_op jit(solution)/shard_map/ppermute | solution.py:334
  12.9 12.3 %collective-permute-start.1 = (bf16[528,128]{1,0:T(8,128)(2,1)}, bf16[528,128]{1,0:T(8,128)(2,1)S(1)}, u32[]{:S(2)}, u32[]{:S(2)}) collective-permute-start(bf16[528,128]{1,0:T(8,128)(2,1)} %get-tuple-element.27), channel_id=1, source_target_pairs={{0,16},{8,24},{16,0},{24,8},{1,17},{9,25},{17,1},{25,9},{2,18},{10... | collective-permute-start | bytes 405512 | tf_op jit(solution)/shard_map/ppermute | solution.py:334
  15.5 9.8 %collective-permute-start.2 = (bf16[528,128]{1,0:T(8,128)(2,1)}, bf16[528,128]{1,0:T(8,128)(2,1)S(1)}, u32[]{:S(2)}, u32[]{:S(2)}) collective-permute-start(bf16[528,128]{1,0:T(8,128)(2,1)} %get-tuple-element.28), channel_id=1, source_target_pairs={{0,24},{8,0},{16,8},{24,16},{1,25},{9,1},{17,9},{25,17},{2,26},{10... | collective-permute-start | bytes 405512 | tf_op jit(solution)/shard_map/ppermute | solution.py:334
  22.2 3.1 %copy-start.9 = (bf16[528,128]{1,0:T(8,128)(2,1)}, bf16[528,128]{1,0:T(8,128)(2,1)S(1)}, u32[]{:S(2)}) copy-start(bf16[528,128]{1,0:T(8,128)(2,1)S(1)} %collective-permute-done.rest_0_) | copy-start | bytes 405508
  25.2 0.9 copy-start
  29.0 12.2 %collective-permute-start.11 = (bf16[4,128,256]{2,1,0:T(8,128)(2,1)}, bf16[4,128,256]{2,1,0:T(8,128)(2,1)S(1)}, u32[]{:S(2)}, u32[]{:S(2)}) collective-permute-start(bf16[4,128,256]{2,1,0:T(8,128)(2,1)} %get-tuple-element.37.rest_0_), channel_id=1, source_target_pairs={{0,6},{1,7},{2,0},{3,1},{4,2},{5,3},{6,4},{7,5},{8,14},{9,15},{10,... | collective-permute-start | bytes 786440 | tf_op jit(solution)/shard_map/ppermute | solution.py:364
  31.6 13.7 %collective-permute-start.9 = (bf16[4,128,256]{2,1,0:T(8,128)(2,1)}, bf16[4,128,256]{2,1,0:T(8,128)(2,1)S(1)}, u32[]{:S(2)}, u32[]{:S(2)}) collective-permute-start(bf16[4,128,256]{2,1,0:T(8,128)(2,1)} %get-tuple-element.37.rest_0_), channel_id=1, source_target_pairs={{0,4},{1,5},{2,6},{3,7},{4,0},{5,1},{6,2},{7,3},{8,12},{9,13},{10,... | collective-permute-start | bytes 786440 | tf_op jit(solution)/shard_map/ppermute | solution.py:364
  32.1 13.1 %collective-permute-start.7 = (bf16[4,128,256]{2,1,0:T(8,128)(2,1)}, bf16[4,128,256]{2,1,0:T(8,128)(2,1)S(1)}, u32[]{:S(2)}, u32[]{:S(2)}) collective-permute-start(bf16[4,128,256]{2,1,0:T(8,128)(2,1)} %get-tuple-element.37.rest_0_), channel_id=1, source_target_pairs={{0,2},{1,3},{2,4},{3,5},{4,6},{5,7},{6,0},{7,1},{8,10},{9,11},{10,... | collective-permute-start | bytes 786440 | tf_op jit(solution)/shard_map/ppermute | solution.py:364
  32.7 8.5 %collective-permute-start.3 = (bf16[512,128]{1,0:T(8,128)(2,1)}, bf16[512,128]{1,0:T(8,128)(2,1)S(1)}, u32[]{:S(2)}, u32[]{:S(2)}) collective-permute-start(bf16[512,128]{1,0:T(8,128)(2,1)} %get-tuple-element.34), channel_id=1, source_target_pairs={{0,8},{8,16},{16,24},{24,0},{1,9},{9,17},{17,25},{25,1},{2,10},{10... | collective-permute-start | bytes 393224 | tf_op jit(solution)/shard_map/ppermute | solution.py:334
  36.0 9.8 %collective-permute-start.4 = (bf16[512,128]{1,0:T(8,128)(2,1)}, bf16[512,128]{1,0:T(8,128)(2,1)S(1)}, u32[]{:S(2)}, u32[]{:S(2)}) collective-permute-start(bf16[512,128]{1,0:T(8,128)(2,1)} %get-tuple-element.35), channel_id=1, source_target_pairs={{0,16},{8,24},{16,0},{24,8},{1,17},{9,25},{17,1},{25,9},{2,18},{10... | collective-permute-start | bytes 393224 | tf_op jit(solution)/shard_map/ppermute | solution.py:334
  41.3 12.0 %copy-start.13 = (bf16[512,128]{1,0:T(8,128)(2,1)}, bf16[512,128]{1,0:T(8,128)(2,1)S(1)}, u32[]{:S(2)}) copy-start(bf16[512,128]{1,0:T(8,128)(2,1)S(1)} %collective-permute-done.3.rest_8_.rest_3_) | copy-start | bytes 393220
  41.3 11.9 %collective-permute-start.6 = (bf16[4,128,256]{2,1,0:T(8,128)(2,1)}, bf16[4,128,256]{2,1,0:T(8,128)(2,1)S(1)}, u32[]{:S(2)}, u32[]{:S(2)}) collective-permute-start(bf16[4,128,256]{2,1,0:T(8,128)(2,1)} %get-tuple-element.37.rest_0_), channel_id=1, source_target_pairs={{0,1},{1,0},{2,3},{3,2},{4,5},{5,4},{6,7},{7,6},{8,9},{9,8},{10,11... | collective-permute-start | bytes 786440 | tf_op jit(solution)/shard_map/ppermute | solution.py:367
  41.3 12.0 %copy-start.1 = (bf16[4,128,256]{2,1,0:T(8,128)(2,1)}, bf16[4,128,256]{2,1,0:T(8,128)(2,1)S(1)}, u32[]{:S(2)}) copy-start(bf16[4,128,256]{2,1,0:T(8,128)(2,1)S(1)} %collective-permute-done.11.rest_6_) | copy-start | bytes 786436
  41.3 11.9 %collective-permute-start.12 = (bf16[4,128,256]{2,1,0:T(8,128)(2,1)S(1)}, bf16[4,128,256]{2,1,0:T(8,128)(2,1)S(1)}, u32[]{:S(2)}, u32[]{:S(2)}) collective-permute-start(bf16[4,128,256]{2,1,0:T(8,128)(2,1)S(1)} %collective-permute-done.11.rest_6_), channel_id=1, source_target_pairs={{0,1},{1,0},{2,3},{3,2},{4,5},{5,4},{6,7},{7,6},{8,9},{9,8},{10,11... | collective-permute-start | bytes 786440 | tf_op jit(solution)/shard_map/ppermute | solution.py:367
  45.3 8.0 %copy-start.2 = (bf16[4,128,256]{2,1,0:T(8,128)(2,1)}, bf16[4,128,256]{2,1,0:T(8,128)(2,1)S(1)}, u32[]{:S(2)}) copy-start(bf16[4,128,256]{2,1,0:T(8,128)(2,1)S(1)} %collective-permute-done.9.rest_4_) | copy-start | bytes 786436
  45.3 7.9 %collective-permute-start.10 = (bf16[4,128,256]{2,1,0:T(8,128)(2,1)S(1)}, bf16[4,128,256]{2,1,0:T(8,128)(2,1)S(1)}, u32[]{:S(2)}, u32[]{:S(2)}) collective-permute-start(bf16[4,128,256]{2,1,0:T(8,128)(2,1)S(1)} %collective-permute-done.9.rest_4_), channel_id=1, source_target_pairs={{0,1},{1,0},{2,3},{3,2},{4,5},{5,4},{6,7},{7,6},{8,9},{9,8},{10,11... | collective-permute-start | bytes 786440 | tf_op jit(solution)/shard_map/ppermute | solution.py:367
  45.3 8.0 %copy-start.3 = (bf16[4,128,256]{2,1,0:T(8,128)(2,1)}, bf16[4,128,256]{2,1,0:T(8,128)(2,1)S(1)}, u32[]{:S(2)}) copy-start(bf16[4,128,256]{2,1,0:T(8,128)(2,1)S(1)} %collective-permute-done.7.rest_2_) | copy-start | bytes 786436
  45.3 7.9 %collective-permute-start.8 = (bf16[4,128,256]{2,1,0:T(8,128)(2,1)S(1)}, bf16[4,128,256]{2,1,0:T(8,128)(2,1)S(1)}, u32[]{:S(2)}, u32[]{:S(2)}) collective-permute-start(bf16[4,128,256]{2,1,0:T(8,128)(2,1)S(1)} %collective-permute-done.7.rest_2_), channel_id=1, source_target_pairs={{0,1},{1,0},{2,3},{3,2},{4,5},{5,4},{6,7},{7,6},{8,9},{9,8},{10,11... | collective-permute-start | bytes 786440 | tf_op jit(solution)/shard_map/ppermute | solution.py:367
  45.8 7.5 %copy-start.14 = (bf16[512,128]{1,0:T(8,128)(2,1)}, bf16[512,128]{1,0:T(8,128)(2,1)S(1)}, u32[]{:S(2)}) copy-start(bf16[512,128]{1,0:T(8,128)(2,1)S(1)} %collective-permute-done.4.rest_9_.rest_4_) | copy-start | bytes 393220
  45.8 7.4 %collective-permute-start.5 = (bf16[512,128]{1,0:T(8,128)(2,1)}, bf16[512,128]{1,0:T(8,128)(2,1)S(1)}, u32[]{:S(2)}, u32[]{:S(2)}) collective-permute-start(bf16[512,128]{1,0:T(8,128)(2,1)} %get-tuple-element.36), channel_id=1, source_target_pairs={{0,24},{8,0},{16,8},{24,16},{1,25},{9,1},{17,9},{25,17},{2,26},{10... | collective-permute-start | bytes 393224 | tf_op jit(solution)/shard_map/ppermute | solution.py:334
  53.2 0.9 copy-start.6
  58.4 12.0 %collective-permute-start.13 = (bf16[256,256]{1,0:T(8,128)(2,1)}, bf16[256,256]{1,0:T(8,128)(2,1)S(1)}, u32[]{:S(2)}, u32[]{:S(2)}) collective-permute-start(bf16[256,256]{1,0:T(8,128)(2,1)} %get-tuple-element.42), channel_id=1, source_target_pairs={{0,8},{8,16},{16,24},{24,0},{1,9},{9,17},{17,25},{25,1},{2,10},{10... | collective-permute-start | bytes 393224 | tf_op jit(solution)/shard_map/ppermute | solution.py:334
  60.2 10.9 %collective-permute-start.14 = (bf16[256,256]{1,0:T(8,128)(2,1)}, bf16[256,256]{1,0:T(8,128)(2,1)S(1)}, u32[]{:S(2)}, u32[]{:S(2)}) collective-permute-start(bf16[256,256]{1,0:T(8,128)(2,1)} %get-tuple-element.43), channel_id=1, source_target_pairs={{0,16},{8,24},{16,0},{24,8},{1,17},{9,25},{17,1},{25,9},{2,18},{10... | collective-permute-start | bytes 393224 | tf_op jit(solution)/shard_map/ppermute | solution.py:334
  62.9 8.3 %collective-permute-start.15 = (bf16[256,256]{1,0:T(8,128)(2,1)}, bf16[256,256]{1,0:T(8,128)(2,1)S(1)}, u32[]{:S(2)}, u32[]{:S(2)}) collective-permute-start(bf16[256,256]{1,0:T(8,128)(2,1)} %get-tuple-element.44), channel_id=1, source_target_pairs={{0,24},{8,0},{16,8},{24,16},{1,25},{9,1},{17,9},{25,17},{2,26},{10... | collective-permute-start | bytes 393224 | tf_op jit(solution)/shard_map/ppermute | solution.py:334
  66.8 4.4 %copy-start.8 = (f32[256,256]{1,0:T(8,128)S(1)}, f32[256,256]{1,0:T(8,128)}, u32[]{:S(2)}) copy-start(f32[256,256]{1,0:T(8,128)} %get-tuple-element.38.rest_8_) | copy-start | bytes 786436
  66.8 24.5 %all-to-all-start.1 = ((bf16[8,128,256]{2,1,0:T(8,128)(2,1)}), bf16[8,128,256]{2,1,0:T(8,128)(2,1)S(1)}, u32[]{:S(2)}, u32[]{:S(2)}) async-start(bf16[8,128,256]{2,1,0:T(8,128)(2,1)} %input_rows.1.rest_6_), calls=%async_computation.1 | async-start | bytes 1048576 | tf_op jit(solution)/shard_map/all_to_all | solution.py:382
  71.2 11.3 %copy-start.12 = (bf16[256,256]{1,0:T(8,128)(2,1)}, bf16[256,256]{1,0:T(8,128)(2,1)S(1)}, u32[]{:S(2)}) copy-start(bf16[256,256]{1,0:T(8,128)(2,1)S(1)} %add_convert_fusion.rest_0_) | copy-start | bytes 393220
  71.2 11.3 %collective-permute-start.18 = (bf16[256,256]{1,0:T(8,128)(2,1)S(1)}, bf16[256,256]{1,0:T(8,128)(2,1)S(1)}, u32[]{:S(2)}, u32[]{:S(2)}) collective-permute-start(bf16[256,256]{1,0:T(8,128)(2,1)S(1)} %add_convert_fusion.rest_0_), channel_id=1, source_target_pairs={{0,24},{8,0},{16,8},{24,16},{1,25},{9,1},{17,9},{25,17},{2,26},{10... | collective-permute-start | bytes 393224 | tf_op jit(solution)/shard_map/ppermute | solution.py:334
  74.2 13.6 %collective-permute-start.17 = (bf16[256,256]{1,0:T(8,128)(2,1)S(1)}, bf16[256,256]{1,0:T(8,128)(2,1)S(1)}, u32[]{:S(2)}, u32[]{:S(2)}) collective-permute-start(bf16[256,256]{1,0:T(8,128)(2,1)S(1)} %add_convert_fusion.rest_0_), channel_id=1, source_target_pairs={{0,16},{8,24},{16,0},{24,8},{1,17},{9,25},{17,1},{25,9},{2,18},{10... | collective-permute-start | bytes 393224 | tf_op jit(solution)/shard_map/ppermute | solution.py:334
  76.0 11.8 %collective-permute-start.16 = (bf16[256,256]{1,0:T(8,128)(2,1)S(1)}, bf16[256,256]{1,0:T(8,128)(2,1)S(1)}, u32[]{:S(2)}, u32[]{:S(2)}) collective-permute-start(bf16[256,256]{1,0:T(8,128)(2,1)S(1)} %add_convert_fusion.rest_0_), channel_id=1, source_target_pairs={{0,8},{8,16},{16,24},{24,0},{1,9},{9,17},{17,25},{25,1},{2,10},{10... | collective-permute-start | bytes 393224 | tf_op jit(solution)/shard_map/ppermute | solution.py:334
  82.6 5.2 %copy-start.16 = (bf16[256,256]{1,0:T(8,128)(2,1)}, bf16[256,256]{1,0:T(8,128)(2,1)S(1)}, u32[]{:S(2)}) copy-start(bf16[256,256]{1,0:T(8,128)(2,1)S(1)} %collective-permute-done.18.rest_3_) | copy-start | bytes 393220
  (8 other events, 5.6 us)

commit v2 on v1

--- a/solution.py
+++ b/solution.py
@@ -6,6 +6,7 @@
 from jax.experimental import pallas as pl
 from jax.experimental.pallas import tpu as pltpu
 from jax.sharding import PartitionSpec as P
+
 
 HEAD_DIM = 64
 PAIR = 2 * HEAD_DIM
@@ -160,7 +161,7 @@
     me = place[0]
     count = seq_devices - 1
     messages = rest[:count]
-    value_ref, before_ref, after_ref = rest[2 * count + 1 : 2 * count + 4]
+    value_ref, before_ref, after_ref = rest[2 * count : 2 * count + 3]
     width = value_ref.shape[2]
     for pair in range(pairs):
         at = lanes(pair)
@@ -297,7 +298,7 @@
                 out_ref[:, block * width : (block + 1) * width] = rest[shift][...].astype(F32)
 
 
-def call(body, shapes, place, *operands, name, waits=(), through=()):
+def call(body, shapes, place, *operands, waits=(), through=()):
     vmem = pl.BlockSpec(memory_space=pltpu.VMEM)
     anywhere = pl.BlockSpec(memory_space=pl.ANY)
     first = 1 + len(operands) + len(waits)
@@ -310,7 +311,6 @@
         + [anywhere] * (len(waits) + len(through)),
         out_specs=[vmem] * len(shapes) + [anywhere] * len(through),
         input_output_aliases={first + i: len(shapes) + i for i in range(len(through))},
-        name=name,
     )(place, *operands, *waits, *through)
 
 
@@ -340,13 +340,13 @@
     read_own = call(
         functools.partial(read_states_kernel, **sizes),
         [((pairs * HEAD_DIM + 2 * pairs, PAIR), BF)] * count,
-        place, query, gate, upstream, name="read_states",
+        place, query, gate, upstream,
     )
     read_other = around(read_own)
     inner, *write_own = call(
         functools.partial(inner_values_kernel, **sizes),
         [((tokens, width), F32)] + [((pairs * HEAD_DIM, PAIR), BF)] * count,
-        place, query, key, value, gate, upstream, name="inner_values",
+        place, query, key, value, gate, upstream,
     )
     input_rows = lax.all_to_all(
         inputs[0].reshape(tokens, row_devices, rows).transpose(1, 2, 0), "dp", 0, 0, tiled=True
@@ -354,9 +354,10 @@
     value_grad, before, after, *write_own = call(
         functools.partial(values_kernel, **sizes),
         [((seq_devices, tokens, columns), BF)] + [((pairs * HEAD_DIM, PAIR), F32)] * 2,
-        place, key, gate, inner, *read_other, name="value_grads",
-        waits=(input_rows,), through=write_own,
-    )
+        place, key, gate, inner, *read_other,
+        through=write_own,
+    )
+    write_other = around(write_own)
     pieces = []
     for shift in range(chips):
         piece = value_grad
@@ -366,17 +367,16 @@
             )
         swapped = lax.ppermute(piece, "dp", [(i, i ^ 1) for i in range(row_devices)])
         pieces += [piece, swapped]
-    write_other = around(write_own)
     partial = call(
         functools.partial(weight_kernel, row_devices=row_devices, seq_devices=seq_devices),
         [((rows, columns), F32)] + [((rows, columns), BF)] * count,
-        place, input_rows, *pieces, name="weight_part", waits=write_other,
+        place, input_rows, *pieces, waits=write_other,
     )
     shares = around(partial[1:])
     (token_rows,) = call(
         functools.partial(inputs_kernel, row_devices=row_devices),
         [((row_devices, tokens, rows), BF)],
-        place, value_weight, *pieces, name="input_rows", waits=partial[:1],
+        place, value_weight, *pieces, waits=partial[:1],
     )
     grad_inputs = (
         lax.all_to_all(token_rows, "dp", 0, 0, tiled=True)
@@ -387,13 +387,14 @@
         functools.partial(rest_kernel, **sizes),
         [((tokens, width), BF)] * 3,
         place, query, key, value, gate, upstream, before, after, *read_other, *write_other,
-        name="other_grads", waits=(token_rows,),
+        waits=(token_rows,),
     )
     share = (partial[0] + sum(part.astype(F32) for part in shares)).astype(BF)
     (grad_weight,) = call(
         functools.partial(join_kernel, seq_devices=seq_devices),
         [((rows, width), F32)],
-        place, share, *around([share] * count), name="join",
+        place, share, *around([share] * count),
+        waits=(grad_inputs,),
     )
     return (grad_queries[None], grad_keys[None], grad_decay[None], grad_inputs, grad_weight)
 

time: 93.1 us -> 87.9 us (0.944)
  starting transfers between devices: 37 us -> 33.6 us
  local copies, waits for them, and re-layouts: 7.06 us -> 6.06 us
  waiting for transfers between devices: 19.7 us -> 18.7 us
    ppermute x3, waiting for transfers between devices: 3.49 us -> 1.32 us  [per_device(): lax.ppermute(value_grad, 'dp', [(i, (i + 2 * shift) % row_devices) for i...]
    ppermute x12, starting transfers between devices: 23.5 us -> 21.3 us  [around(): lax.ppermute(message, 'sp', [(i, (i + shift) % seq_devices) for i in rang...]
    unnamed x40 -> x49, local copies, waits for them, and re-layouts: 6.79 us -> 4.73 us
    all_to_all x1, starting transfers between devices: 5.2 us -> 3.81 us  [per_device(): lax.all_to_all(inputs[0].reshape(tokens, row_devices, rows).transpose(1,...]
    ppermute x12, waiting for transfers between devices: 16.2 us -> 17.4 us  [around(): lax.ppermute(message, 'sp', [(i, (i + shift) % seq_devices) for i in rang...]
    reshape x0 -> x1, local copies, waits for them, and re-layouts: none -> 1.03 us  [per_device(): grad_inputs = lax.all_to_all(token_rows, 'dp', 0, 0, tiled=True).transpos...]
  transfers between devices with their start and end apart: 21 -> 21, of which waited for: 7 -> 7; matrix products, arithmetic and copies ran while one was open for 1% -> 3% of each run, Pallas kernels for 23% -> 18%
where the time goes in v2:
time: 87.9 us; the launch traced here: 87.4 us
  starting transfers between devices  33.6 us (38%)
  Pallas kernels  27.5 us (31%)
  waiting for transfers between devices  18.7 us (21%)
  local copies, waits for them, and re-layouts  6.06 us (7%)
    pallas_call x7, Pallas kernels, call(): pl.pallas_call(body, out_shape=[jax.ShapeDtypeStruct(shape, dtype) for sh...  27.5 us
    ppermute x12, starting transfers between devices, around(): lax.ppermute(message, 'sp', [(i, (i + shift) % seq_devices) for i in rang...  21.3 us
    ppermute x12, waiting for transfers between devices, around(): lax.ppermute(message, 'sp', [(i, (i + shift) % seq_devices) for i in rang...  17.4 us
    unnamed x49, local copies, waits for them, and re-layouts  4.73 us
    all_to_all x1, starting transfers between devices, per_device(): lax.all_to_all(token_rows, 'dp', 0, 0, tiled=True).transpose(1, 0, 2)  3.92 us
    all_to_all x1, starting transfers between devices, per_device(): lax.all_to_all(inputs[0].reshape(tokens, row_devices, rows).transpose(1,...  3.81 us
    ppermute x3, starting transfers between devices, per_device(): lax.ppermute(value_grad, 'dp', [(i, (i + 2 * shift) % row_devices) for i...  3.54 us
  transfers between devices with their start and end apart: 21, of which 7 were waited for; matrix products, arithmetic and copies ran while one was open for 3% of the time, Pallas kernels for 18%

profile of v2, /device:TPU:0, one launch (start us, length us, event | category | flops | bytes accessed | tf_op | source)
XLA Modules:
  0.0 87.4 jit_solution(13857103623828928340)
XLA Ops:
  0.6 0.7 pad_add_fusion.place
  1.3 2.9 %shard_map.111 = (bf16[528,128]{1,0:T(8,128)(2,1)}, bf16[528,128]{1,0:T(8,128)(2,1)}, bf16[528,128]{1,0:T(8,128)(2,1)}) custom-call(s32[2]{0:T(128)} %pad_add_fusion.place, bf16[128,1024]{1,0:T(8,128)(2,1)} %bitcast.18, bf16[128,1024]{1,0:T(8,128)(2,1)} %bitcast.14, bf16[128,1024]{1,0:T(8,128)(2,1)} %bitcast.24), custom_call_target="tpu_custom_call" | custom-call | tf_op jit(solution)/shard_map/pallas_call | solution.py:305
  4.2 3.1 %collective-permute-start = (bf16[528,128]{1,0:T(8,128)(2,1)}, bf16[528,128]{1,0:T(8,128)(2,1)S(1)}, u32[]{:S(2)}, u32[]{:S(2)}) collective-permute-start(bf16[528,128]{1,0:T(8,128)(2,1)} %get-tuple-element.26), channel_id=1, source_target_pairs={{0,8},{8,16},{16,24},{24,0},{1,9},{9,17},{17,25},{25,1},{2,10},{10... | collective-permute-start | bytes 405512 | tf_op jit(solution)/shard_map/ppermute | solution.py:334
  7.2 2.6 %collective-permute-start.1 = (bf16[528,128]{1,0:T(8,128)(2,1)}, bf16[528,128]{1,0:T(8,128)(2,1)S(1)}, u32[]{:S(2)}, u32[]{:S(2)}) collective-permute-start(bf16[528,128]{1,0:T(8,128)(2,1)} %get-tuple-element.27), channel_id=1, source_target_pairs={{0,16},{8,24},{16,0},{24,8},{1,17},{9,25},{17,1},{25,9},{2,18},{10... | collective-permute-start | bytes 405512 | tf_op jit(solution)/shard_map/ppermute | solution.py:334
  9.8 1.3 %collective-permute-start.2 = (bf16[528,128]{1,0:T(8,128)(2,1)}, bf16[528,128]{1,0:T(8,128)(2,1)S(1)}, u32[]{:S(2)}, u32[]{:S(2)}) collective-permute-start(bf16[528,128]{1,0:T(8,128)(2,1)} %get-tuple-element.28), channel_id=1, source_target_pairs={{0,24},{8,0},{16,8},{24,16},{1,25},{9,1},{17,9},{25,17},{2,26},{10... | collective-permute-start | bytes 405512 | tf_op jit(solution)/shard_map/ppermute | solution.py:334
  11.2 5.3 %shard_map.110 = (f32[128,1024]{1,0:T(8,128)}, bf16[512,128]{1,0:T(8,128)(2,1)}, bf16[512,128]{1,0:T(8,128)(2,1)}, bf16[512,128]{1,0:T(8,128)(2,1)}) custom-call(s32[2]{0:T(128)} %pad_add_fusion.place, bf16[128,1024]{1,0:T(8,128)(2,1)} %bitcast.19, bf16[128,1024]{1,0:T(8,128)(2,1)} %bitcast.21, bf16[128,1024]{1,0:T(8,128)(2,1)} %bitcast.28, ...), custom_call_target="tpu_custom_call" | custom-call | tf_op jit(solution)/shard_map/pallas_call | solution.py:305
  16.5 2.4 %collective-permute-done.1.rest_1_ = bf16[528,128]{1,0:T(8,128)(2,1)S(1)} collective-permute-done((bf16[528,128]{1,0:T(8,128)(2,1)}, bf16[528,128]{1,0:T(8,128)(2,1)S(1)}, u32[]{:S(2)}, u32[]{:S(2)}) %collective-permute-start.1) | collective-permute-done | bytes 135200 | tf_op jit(solution)/shard_map/ppermute | solution.py:334
  18.9 0.6 copy-done.11
  19.6 3.0 %shard_map.112 = (bf16[4,128,256]{2,1,0:T(8,128)(2,1)}, f32[512,128]{1,0:T(8,128)}, f32[512,128]{1,0:T(8,128)}, bf16[512,128]{1,0:T(8,128)(2,1)}, bf16[512,128]{1,0:T(8,128)(2,1)}, /*index=5*/bf16[512,128]{1,0:T(8,128)(2,1)}) custom-call(s32[2]{0:T(128)} %pad_add_fusion.place, ...), custom_call_target="tpu_custom_call", output_to_operand_aliasing={{3}: (7, {}), {4}: (8, {}), {5}: (9, {})} | custom-call | tf_op jit(solution)/shard_map/pallas_call | solution.py:305
  22.6 2.4 %collective-permute-start.11 = (bf16[4,128,256]{2,1,0:T(8,128)(2,1)}, bf16[4,128,256]{2,1,0:T(8,128)(2,1)S(1)}, u32[]{:S(2)}, u32[]{:S(2)}) collective-permute-start(bf16[4,128,256]{2,1,0:T(8,128)(2,1)} %get-tuple-element.37.rest_0_), channel_id=1, source_target_pairs={{0,6},{1,7},{2,0},{3,1},{4,2},{5,3},{6,4},{7,5},{8,14},{9,15},{10,... | collective-permute-start | bytes 786440 | tf_op jit(solution)/shard_map/ppermute | solution.py:365
  26.2 1.0 %copy.15 = bf16[1,128,2048]{1,2,0:T(8,128)(2,1)} copy(bf16[1,128,2048]{2,1,0:T(8,128)(2,1)S(1)} %copy-done.13) | data formatting | bytes 1048576 | tf_op args[0]
  27.2 3.8 %all-to-all-start = ((bf16[8,256,128]{2,1,0:T(8,128)(2,1)}), bf16[8,256,128]{2,1,0:T(8,128)(2,1)S(1)}, u32[]{:S(2)}, u32[]{:S(2)}) async-start(bf16[8,256,128]{2,1,0:T(8,128)(2,1)} %bitcast.8), calls=%async_computation | async-start | bytes 1048576 | tf_op jit(solution)/shard_map/all_to_all | solution.py:351
  31.0 3.4 %collective-permute-start.3 = (bf16[512,128]{1,0:T(8,128)(2,1)S(1)}, bf16[512,128]{1,0:T(8,128)(2,1)S(1)}, u32[]{:S(2)}, u32[]{:S(2)}) collective-permute-start(bf16[512,128]{1,0:T(8,128)(2,1)S(1)} %copy-done.21), channel_id=1, source_target_pairs={{0,8},{8,16},{16,24},{24,0},{1,9},{9,17},{17,25},{25,1},{2,10},{10... | collective-permute-start | bytes 393224 | tf_op jit(solution)/shard_map/ppermute | solution.py:334
  34.3 1.7 %collective-permute-start.4 = (bf16[512,128]{1,0:T(8,128)(2,1)S(1)}, bf16[512,128]{1,0:T(8,128)(2,1)S(1)}, u32[]{:S(2)}, u32[]{:S(2)}) collective-permute-start(bf16[512,128]{1,0:T(8,128)(2,1)S(1)} %copy-done.22), channel_id=1, source_target_pairs={{0,16},{8,24},{16,0},{24,8},{1,17},{9,25},{17,1},{25,9},{2,18},{10... | collective-permute-start | bytes 393224 | tf_op jit(solution)/shard_map/ppermute | solution.py:334
  36.0 3.9 %collective-permute-done.3.rest_8_.rest_3_ = bf16[512,128]{1,0:T(8,128)(2,1)S(1)} collective-permute-done((bf16[512,128]{1,0:T(8,128)(2,1)S(1)}, bf16[512,128]{1,0:T(8,128)(2,1)S(1)}, u32[]{:S(2)}, u32[]{:S(2)}) %collective-permute-start.3) | collective-permute-done | bytes 131104 | tf_op jit(solution)/shard_map/ppermute | solution.py:334
  40.4 1.3 %collective-permute-done.9.rest_4_ = bf16[4,128,256]{2,1,0:T(8,128)(2,1)S(1)} collective-permute-done((bf16[4,128,256]{2,1,0:T(8,128)(2,1)}, bf16[4,128,256]{2,1,0:T(8,128)(2,1)S(1)}, u32[]{:S(2)}, u32[]{:S(2)}) %collective-permute-start.9) | collective-permute-done | bytes 262176 | tf_op jit(solution)/shard_map/ppermute | solution.py:365
  42.3 2.9 %collective-permute-done.4.rest_9_.rest_4_ = bf16[512,128]{1,0:T(8,128)(2,1)S(1)} collective-permute-done((bf16[512,128]{1,0:T(8,128)(2,1)S(1)}, bf16[512,128]{1,0:T(8,128)(2,1)S(1)}, u32[]{:S(2)}, u32[]{:S(2)}) %collective-permute-start.4) | collective-permute-done | bytes 131104 | tf_op jit(solution)/shard_map/ppermute | solution.py:334
  45.2 1.2 %collective-permute-start.5 = (bf16[512,128]{1,0:T(8,128)(2,1)S(1)}, bf16[512,128]{1,0:T(8,128)(2,1)S(1)}, u32[]{:S(2)}, u32[]{:S(2)}) collective-permute-start(bf16[512,128]{1,0:T(8,128)(2,1)S(1)} %copy-done.23), channel_id=1, source_target_pairs={{0,24},{8,0},{16,8},{24,16},{1,25},{9,1},{17,9},{25,17},{2,26},{10... | collective-permute-start | bytes 393224 | tf_op jit(solution)/shard_map/ppermute | solution.py:334
  46.4 4.2 %collective-permute-done.5.rest_10_.rest_5_ = bf16[512,128]{1,0:T(8,128)(2,1)S(1)} collective-permute-done((bf16[512,128]{1,0:T(8,128)(2,1)S(1)}, bf16[512,128]{1,0:T(8,128)(2,1)S(1)}, u32[]{:S(2)}, u32[]{:S(2)}) %collective-permute-start.5) | collective-permute-done | bytes 131104 | tf_op jit(solution)/shard_map/ppermute | solution.py:334
  51.7 0.7 copy-done.8
  52.4 3.6 %shard_map.113 = (f32[256,256]{1,0:T(8,128)}, bf16[256,256]{1,0:T(8,128)(2,1)}, bf16[256,256]{1,0:T(8,128)(2,1)}, bf16[256,256]{1,0:T(8,128)(2,1)}) custom-call(s32[2]{0:T(128)} %pad_add_fusion.place, bf16[8,256,128]{2,1,0:T(8,128)(2,1)} %copy-done, bf16[4,128,256]{2,1,0:T(8,128)(2,1)} %get-tuple-element.37.rest_0_, bf16[4,128,256]{2,1,0:T(8,128)(2,1)} %copy-done.5, ...), custom_call_target="tpu_custom_call" | custom-call | tf_op jit(solution)/shard_map/pallas_call | solution.py:305
  56.5 2.9 %collective-permute-start.14 = (bf16[256,256]{1,0:T(8,128)(2,1)}, bf16[256,256]{1,0:T(8,128)(2,1)S(1)}, u32[]{:S(2)}, u32[]{:S(2)}) collective-permute-start(bf16[256,256]{1,0:T(8,128)(2,1)} %get-tuple-element.43), channel_id=1, source_target_pairs={{0,16},{8,24},{16,0},{24,8},{1,17},{9,25},{17,1},{25,9},{2,18},{10... | collective-permute-start | bytes 393224 | tf_op jit(solution)/shard_map/ppermute | solution.py:334
  59.9 3.9 %shard_map.114.rest_6_ = bf16[8,128,256]{2,1,0:T(8,128)(2,1)} custom-call(s32[2]{0:T(128)} %pad_add_fusion.place, bf16[256,1024]{1,0:T(8,128)(2,1)} %w_ref.1, bf16[4,128,256]{2,1,0:T(8,128)(2,1)} %get-tuple-element.37.rest_0_, bf16[4,128,256]{2,1,0:T(8,128)(2,1)} %copy-done.5, bf16[4,128,256]{2,1,0:T(8,128)(2,1)} %copy-done.4, ...), custom_call_target="tpu_custom_call" | custom-call | tf_op jit(solution)/shard_map/pallas_call | solution.py:305
  63.8 3.9 %all-to-all-start.1 = ((bf16[8,128,256]{2,1,0:T(8,128)(2,1)}), bf16[8,128,256]{2,1,0:T(8,128)(2,1)S(1)}, u32[]{:S(2)}, u32[]{:S(2)}) async-start(bf16[8,128,256]{2,1,0:T(8,128)(2,1)} %shard_map.114.rest_6_), calls=%async_computation.1 | async-start | bytes 1048576 | tf_op jit(solution)/shard_map/all_to_all | solution.py:382
  68.4 2.6 %collective-permute-start.18 = (bf16[256,256]{1,0:T(8,128)(2,1)S(1)}, bf16[256,256]{1,0:T(8,128)(2,1)S(1)}, u32[]{:S(2)}, u32[]{:S(2)}) collective-permute-start(bf16[256,256]{1,0:T(8,128)(2,1)S(1)} %add_convert_fusion.rest_0_), channel_id=1, source_target_pairs={{0,24},{8,0},{16,8},{24,16},{1,25},{9,1},{17,9},{25,17},{2,26},{10... | collective-permute-start | bytes 393224 | tf_op jit(solution)/shard_map/ppermute | solution.py:334
  71.0 1.6 %collective-permute-start.17 = (bf16[256,256]{1,0:T(8,128)(2,1)S(1)}, bf16[256,256]{1,0:T(8,128)(2,1)S(1)}, u32[]{:S(2)}, u32[]{:S(2)}) collective-permute-start(bf16[256,256]{1,0:T(8,128)(2,1)S(1)} %add_convert_fusion.rest_0_), channel_id=1, source_target_pairs={{0,16},{8,24},{16,0},{24,8},{1,17},{9,25},{17,1},{25,9},{2,18},{10... | collective-permute-start | bytes 393224 | tf_op jit(solution)/shard_map/ppermute | solution.py:334
  72.7 6.6 %shard_map.115 = (bf16[128,1024]{1,0:T(8,128)(2,1)}, bf16[128,1024]{1,0:T(8,128)(2,1)}, bf16[128,1024]{1,0:T(8,128)(2,1)}) custom-call(s32[2]{0:T(128)} %pad_add_fusion.place, bf16[128,1024]{1,0:T(8,128)(2,1)} %bitcast.20, bf16[128,1024]{1,0:T(8,128)(2,1)} %bitcast.23, bf16[128,1024]{1,0:T(8,128)(2,1)} %bitcast.29, bf16[128,1024]{1,0:T(8,128)(2,1)} %bitcast.17, ...), custom_call_target="tpu_custom_call" | custom-call | tf_op jit(solution)/shard_map/pallas_call | solution.py:305
  79.6 1.0 %reshape.13.rest_4_ = bf16[1,128,2048]{2,1,0:T(8,128)(2,1)} reshape(bf16[128,8,256]{2,1,0:T(8,128)(2,1)S(1)} %copy.16) | data formatting | bytes 1048576 | tf_op jit(solution)/shard_map/reshape | solution.py:384
  80.6 3.3 %collective-permute-done.17.rest_2_ = bf16[256,256]{1,0:T(8,128)(2,1)S(1)} collective-permute-done((bf16[256,256]{1,0:T(8,128)(2,1)S(1)}, bf16[256,256]{1,0:T(8,128)(2,1)S(1)}, u32[]{:S(2)}, u32[]{:S(2)}) %collective-permute-start.17) | collective-permute-done | bytes 131104 | tf_op jit(solution)/shard_map/ppermute | solution.py:334
  83.9 0.6 copy-done.19
  84.6 0.6 copy-done.20
  85.2 2.2 %shard_map.116 = f32[256,1024]{1,0:T(8,128)} custom-call(s32[2]{0:T(128)} %pad_add_fusion.place, bf16[256,256]{1,0:T(8,128)(2,1)} %copy-done.14, bf16[256,256]{1,0:T(8,128)(2,1)} %copy-done.20, bf16[256,256]{1,0:T(8,128)(2,1)} %copy-done.19, bf16[256,256]{1,0:T(8,128)(2,1)} %copy-done.18, bf16[1,128,2048]{2,1,0:T(8,128)(2,1)} %reshape.13.rest_4_), custom_call_target="tpu_custom_call" | custom-call | tf_op jit(solution)/shard_map/pallas_call | solution.py:305
  (70 shorter events, 5.1 us)
Async XLA Ops:
  4.2 12.3 %collective-permute-start = (bf16[528,128]{1,0:T(8,128)(2,1)}, bf16[528,128]{1,0:T(8,128)(2,1)S(1)}, u32[]{:S(2)}, u32[]{:S(2)}) collective-permute-start(bf16[528,128]{1,0:T(8,128)(2,1)} %get-tuple-element.26), channel_id=1, source_target_pairs={{0,8},{8,16},{16,24},{24,0},{1,9},{9,17},{17,25},{25,1},{2,10},{10... | collective-permute-start | bytes 405512 | tf_op jit(solution)/shard_map/ppermute | solution.py:334
  7.2 11.7 %collective-permute-start.1 = (bf16[528,128]{1,0:T(8,128)(2,1)}, bf16[528,128]{1,0:T(8,128)(2,1)S(1)}, u32[]{:S(2)}, u32[]{:S(2)}) collective-permute-start(bf16[528,128]{1,0:T(8,128)(2,1)} %get-tuple-element.27), channel_id=1, source_target_pairs={{0,16},{8,24},{16,0},{24,8},{1,17},{9,25},{17,1},{25,9},{2,18},{10... | collective-permute-start | bytes 405512 | tf_op jit(solution)/shard_map/ppermute | solution.py:334
  9.8 9.1 %collective-permute-start.2 = (bf16[528,128]{1,0:T(8,128)(2,1)}, bf16[528,128]{1,0:T(8,128)(2,1)S(1)}, u32[]{:S(2)}, u32[]{:S(2)}) collective-permute-start(bf16[528,128]{1,0:T(8,128)(2,1)} %get-tuple-element.28), channel_id=1, source_target_pairs={{0,24},{8,0},{16,8},{24,16},{1,25},{9,1},{17,9},{25,17},{2,26},{10... | collective-permute-start | bytes 405512 | tf_op jit(solution)/shard_map/ppermute | solution.py:334
  19.6 6.5 %copy-start.13 = (bf16[1,128,2048]{2,1,0:T(8,128)(2,1)S(1)}, bf16[1,128,2048]{2,1,0:T(8,128)(2,1)}, u32[]{:S(2)}) copy-start(bf16[1,128,2048]{2,1,0:T(8,128)(2,1)} %param.7) | copy-start | bytes 1572868
  22.6 17.3 %collective-permute-start.11 = (bf16[4,128,256]{2,1,0:T(8,128)(2,1)}, bf16[4,128,256]{2,1,0:T(8,128)(2,1)S(1)}, u32[]{:S(2)}, u32[]{:S(2)}) collective-permute-start(bf16[4,128,256]{2,1,0:T(8,128)(2,1)} %get-tuple-element.37.rest_0_), channel_id=1, source_target_pairs={{0,6},{1,7},{2,0},{3,1},{4,2},{5,3},{6,4},{7,5},{8,14},{9,15},{10,... | collective-permute-start | bytes 786440 | tf_op jit(solution)/shard_map/ppermute | solution.py:365
  25.1 16.7 %collective-permute-start.9 = (bf16[4,128,256]{2,1,0:T(8,128)(2,1)}, bf16[4,128,256]{2,1,0:T(8,128)(2,1)S(1)}, u32[]{:S(2)}, u32[]{:S(2)}) collective-permute-start(bf16[4,128,256]{2,1,0:T(8,128)(2,1)} %get-tuple-element.37.rest_0_), channel_id=1, source_target_pairs={{0,4},{1,5},{2,6},{3,7},{4,0},{5,1},{6,2},{7,3},{8,12},{9,13},{10,... | collective-permute-start | bytes 786440 | tf_op jit(solution)/shard_map/ppermute | solution.py:365
  25.6 16.2 %collective-permute-start.7 = (bf16[4,128,256]{2,1,0:T(8,128)(2,1)}, bf16[4,128,256]{2,1,0:T(8,128)(2,1)S(1)}, u32[]{:S(2)}, u32[]{:S(2)}) collective-permute-start(bf16[4,128,256]{2,1,0:T(8,128)(2,1)} %get-tuple-element.37.rest_0_), channel_id=1, source_target_pairs={{0,2},{1,3},{2,4},{3,5},{4,6},{5,7},{6,0},{7,1},{8,10},{9,11},{10,... | collective-permute-start | bytes 786440 | tf_op jit(solution)/shard_map/ppermute | solution.py:365
  27.2 7.2 %copy-start.22 = (bf16[512,128]{1,0:T(8,128)(2,1)S(1)}, bf16[512,128]{1,0:T(8,128)(2,1)}, u32[]{:S(2)}) copy-start(bf16[512,128]{1,0:T(8,128)(2,1)} %get-tuple-element.35) | copy-start | bytes 393220
  27.2 12.8 %copy-start.1 = (bf16[4,128,256]{2,1,0:T(8,128)(2,1)S(1)}, bf16[4,128,256]{2,1,0:T(8,128)(2,1)}, u32[]{:S(2)}) copy-start(bf16[4,128,256]{2,1,0:T(8,128)(2,1)} %get-tuple-element.37.rest_0_) | copy-start | bytes 786436
  27.2 18.0 %copy-start.23 = (bf16[512,128]{1,0:T(8,128)(2,1)S(1)}, bf16[512,128]{1,0:T(8,128)(2,1)}, u32[]{:S(2)}) copy-start(bf16[512,128]{1,0:T(8,128)(2,1)} %get-tuple-element.36) | copy-start | bytes 393220
  27.2 23.5 %all-to-all-start = ((bf16[8,256,128]{2,1,0:T(8,128)(2,1)}), bf16[8,256,128]{2,1,0:T(8,128)(2,1)S(1)}, u32[]{:S(2)}, u32[]{:S(2)}) async-start(bf16[8,256,128]{2,1,0:T(8,128)(2,1)} %bitcast.8), calls=%async_computation | async-start | bytes 1048576 | tf_op jit(solution)/shard_map/all_to_all | solution.py:351
  31.0 8.9 %collective-permute-start.3 = (bf16[512,128]{1,0:T(8,128)(2,1)S(1)}, bf16[512,128]{1,0:T(8,128)(2,1)S(1)}, u32[]{:S(2)}, u32[]{:S(2)}) collective-permute-start(bf16[512,128]{1,0:T(8,128)(2,1)S(1)} %copy-done.21), channel_id=1, source_target_pairs={{0,8},{8,16},{16,24},{24,0},{1,9},{9,17},{17,25},{25,1},{2,10},{10... | collective-permute-start | bytes 393224 | tf_op jit(solution)/shard_map/ppermute | solution.py:334
  34.3 10.9 %collective-permute-start.4 = (bf16[512,128]{1,0:T(8,128)(2,1)S(1)}, bf16[512,128]{1,0:T(8,128)(2,1)S(1)}, u32[]{:S(2)}, u32[]{:S(2)}) collective-permute-start(bf16[512,128]{1,0:T(8,128)(2,1)S(1)} %copy-done.22), channel_id=1, source_target_pairs={{0,16},{8,24},{16,0},{24,8},{1,17},{9,25},{17,1},{25,9},{2,18},{10... | collective-permute-start | bytes 393224 | tf_op jit(solution)/shard_map/ppermute | solution.py:334
  39.9 10.8 %copy-start.15 = (bf16[512,128]{1,0:T(8,128)(2,1)}, bf16[512,128]{1,0:T(8,128)(2,1)S(1)}, u32[]{:S(2)}) copy-start(bf16[512,128]{1,0:T(8,128)(2,1)S(1)} %collective-permute-done.3.rest_8_.rest_3_) | copy-start | bytes 393220
  39.9 10.7 %collective-permute-start.6 = (bf16[4,128,256]{2,1,0:T(8,128)(2,1)S(1)}, bf16[4,128,256]{2,1,0:T(8,128)(2,1)S(1)}, u32[]{:S(2)}, u32[]{:S(2)}) collective-permute-start(bf16[4,128,256]{2,1,0:T(8,128)(2,1)S(1)} %copy-done.1), channel_id=1, source_target_pairs={{0,1},{1,0},{2,3},{3,2},{4,5},{5,4},{6,7},{7,6},{8,9},{9,8},{10,11... | collective-permute-start | bytes 786440 | tf_op jit(solution)/shard_map/ppermute | solution.py:368
  39.9 10.8 %copy-start.2 = (bf16[4,128,256]{2,1,0:T(8,128)(2,1)}, bf16[4,128,256]{2,1,0:T(8,128)(2,1)S(1)}, u32[]{:S(2)}) copy-start(bf16[4,128,256]{2,1,0:T(8,128)(2,1)S(1)} %collective-permute-done.11.rest_6_) | copy-start | bytes 786436
  40.0 10.7 %collective-permute-start.12 = (bf16[4,128,256]{2,1,0:T(8,128)(2,1)S(1)}, bf16[4,128,256]{2,1,0:T(8,128)(2,1)S(1)}, u32[]{:S(2)}, u32[]{:S(2)}) collective-permute-start(bf16[4,128,256]{2,1,0:T(8,128)(2,1)S(1)} %collective-permute-done.11.rest_6_), channel_id=1, source_target_pairs={{0,1},{1,0},{2,3},{3,2},{4,5},{5,4},{6,7},{7,6},{8,9},{9,8},{10,11... | collective-permute-start | bytes 786440 | tf_op jit(solution)/shard_map/ppermute | solution.py:368
  41.8 9.0 %copy-start.3 = (bf16[4,128,256]{2,1,0:T(8,128)(2,1)}, bf16[4,128,256]{2,1,0:T(8,128)(2,1)S(1)}, u32[]{:S(2)}) copy-start(bf16[4,128,256]{2,1,0:T(8,128)(2,1)S(1)} %collective-permute-done.9.rest_4_) | copy-start | bytes 786436
  41.8 8.9 %collective-permute-start.10 = (bf16[4,128,256]{2,1,0:T(8,128)(2,1)S(1)}, bf16[4,128,256]{2,1,0:T(8,128)(2,1)S(1)}, u32[]{:S(2)}, u32[]{:S(2)}) collective-permute-start(bf16[4,128,256]{2,1,0:T(8,128)(2,1)S(1)} %collective-permute-done.9.rest_4_), channel_id=1, source_target_pairs={{0,1},{1,0},{2,3},{3,2},{4,5},{5,4},{6,7},{7,6},{8,9},{9,8},{10,11... | collective-permute-start | bytes 786440 | tf_op jit(solution)/shard_map/ppermute | solution.py:368
  41.8 9.0 %copy-start.4 = (bf16[4,128,256]{2,1,0:T(8,128)(2,1)}, bf16[4,128,256]{2,1,0:T(8,128)(2,1)S(1)}, u32[]{:S(2)}) copy-start(bf16[4,128,256]{2,1,0:T(8,128)(2,1)S(1)} %collective-permute-done.7.rest_2_) | copy-start | bytes 786436
  41.8 8.9 %collective-permute-start.8 = (bf16[4,128,256]{2,1,0:T(8,128)(2,1)S(1)}, bf16[4,128,256]{2,1,0:T(8,128)(2,1)S(1)}, u32[]{:S(2)}, u32[]{:S(2)}) collective-permute-start(bf16[4,128,256]{2,1,0:T(8,128)(2,1)S(1)} %collective-permute-done.7.rest_2_), channel_id=1, source_target_pairs={{0,1},{1,0},{2,3},{3,2},{4,5},{5,4},{6,7},{7,6},{8,9},{9,8},{10,11... | collective-permute-start | bytes 786440 | tf_op jit(solution)/shard_map/ppermute | solution.py:368
  45.2 5.6 %copy-start.16 = (bf16[512,128]{1,0:T(8,128)(2,1)}, bf16[512,128]{1,0:T(8,128)(2,1)S(1)}, u32[]{:S(2)}) copy-start(bf16[512,128]{1,0:T(8,128)(2,1)S(1)} %collective-permute-done.4.rest_9_.rest_4_) | copy-start | bytes 393220
  45.2 5.4 %collective-permute-start.5 = (bf16[512,128]{1,0:T(8,128)(2,1)S(1)}, bf16[512,128]{1,0:T(8,128)(2,1)S(1)}, u32[]{:S(2)}, u32[]{:S(2)}) collective-permute-start(bf16[512,128]{1,0:T(8,128)(2,1)S(1)} %copy-done.23), channel_id=1, source_target_pairs={{0,24},{8,0},{16,8},{24,16},{1,25},{9,1},{17,9},{25,17},{2,26},{10... | collective-permute-start | bytes 393224 | tf_op jit(solution)/shard_map/ppermute | solution.py:334
  56.1 11.7 %collective-permute-start.13 = (bf16[256,256]{1,0:T(8,128)(2,1)}, bf16[256,256]{1,0:T(8,128)(2,1)S(1)}, u32[]{:S(2)}, u32[]{:S(2)}) collective-permute-start(bf16[256,256]{1,0:T(8,128)(2,1)} %get-tuple-element.42), channel_id=1, source_target_pairs={{0,8},{8,16},{16,24},{24,0},{1,9},{9,17},{17,25},{25,1},{2,10},{10... | collective-permute-start | bytes 393224 | tf_op jit(solution)/shard_map/ppermute | solution.py:334
  56.5 11.8 %collective-permute-start.14 = (bf16[256,256]{1,0:T(8,128)(2,1)}, bf16[256,256]{1,0:T(8,128)(2,1)S(1)}, u32[]{:S(2)}, u32[]{:S(2)}) collective-permute-start(bf16[256,256]{1,0:T(8,128)(2,1)} %get-tuple-element.43), channel_id=1, source_target_pairs={{0,16},{8,24},{16,0},{24,8},{1,17},{9,25},{17,1},{25,9},{2,18},{10... | collective-permute-start | bytes 393224 | tf_op jit(solution)/shard_map/ppermute | solution.py:334
  59.5 8.9 %collective-permute-start.15 = (bf16[256,256]{1,0:T(8,128)(2,1)}, bf16[256,256]{1,0:T(8,128)(2,1)S(1)}, u32[]{:S(2)}, u32[]{:S(2)}) collective-permute-start(bf16[256,256]{1,0:T(8,128)(2,1)} %get-tuple-element.44), channel_id=1, source_target_pairs={{0,24},{8,0},{16,8},{24,16},{1,25},{9,1},{17,9},{25,17},{2,26},{10... | collective-permute-start | bytes 393224 | tf_op jit(solution)/shard_map/ppermute | solution.py:334
  63.8 4.6 %copy-start.9 = (f32[256,256]{1,0:T(8,128)S(1)}, f32[256,256]{1,0:T(8,128)}, u32[]{:S(2)}) copy-start(f32[256,256]{1,0:T(8,128)} %get-tuple-element.38.rest_8_) | copy-start | bytes 786436
  63.8 15.5 %all-to-all-start.1 = ((bf16[8,128,256]{2,1,0:T(8,128)(2,1)}), bf16[8,128,256]{2,1,0:T(8,128)(2,1)S(1)}, u32[]{:S(2)}, u32[]{:S(2)}) async-start(bf16[8,128,256]{2,1,0:T(8,128)(2,1)} %shard_map.114.rest_6_), calls=%async_computation.1 | async-start | bytes 1048576 | tf_op jit(solution)/shard_map/all_to_all | solution.py:382
  68.4 10.8 %copy-start.14 = (bf16[256,256]{1,0:T(8,128)(2,1)}, bf16[256,256]{1,0:T(8,128)(2,1)S(1)}, u32[]{:S(2)}) copy-start(bf16[256,256]{1,0:T(8,128)(2,1)S(1)} %add_convert_fusion.rest_0_) | copy-start | bytes 393220
  68.4 12.2 %collective-permute-start.18 = (bf16[256,256]{1,0:T(8,128)(2,1)S(1)}, bf16[256,256]{1,0:T(8,128)(2,1)S(1)}, u32[]{:S(2)}, u32[]{:S(2)}) collective-permute-start(bf16[256,256]{1,0:T(8,128)(2,1)S(1)} %add_convert_fusion.rest_0_), channel_id=1, source_target_pairs={{0,24},{8,0},{16,8},{24,16},{1,25},{9,1},{17,9},{25,17},{2,26},{10... | collective-permute-start | bytes 393224 | tf_op jit(solution)/shard_map/ppermute | solution.py:334
  71.0 12.9 %collective-permute-start.17 = (bf16[256,256]{1,0:T(8,128)(2,1)S(1)}, bf16[256,256]{1,0:T(8,128)(2,1)S(1)}, u32[]{:S(2)}, u32[]{:S(2)}) collective-permute-start(bf16[256,256]{1,0:T(8,128)(2,1)S(1)} %add_convert_fusion.rest_0_), channel_id=1, source_target_pairs={{0,16},{8,24},{16,0},{24,8},{1,17},{9,25},{17,1},{25,9},{2,18},{10... | collective-permute-start | bytes 393224 | tf_op jit(solution)/shard_map/ppermute | solution.py:334
  72.7 11.3 %collective-permute-start.16 = (bf16[256,256]{1,0:T(8,128)(2,1)S(1)}, bf16[256,256]{1,0:T(8,128)(2,1)S(1)}, u32[]{:S(2)}, u32[]{:S(2)}) collective-permute-start(bf16[256,256]{1,0:T(8,128)(2,1)S(1)} %add_convert_fusion.rest_0_), channel_id=1, source_target_pairs={{0,8},{8,16},{16,24},{24,0},{1,9},{9,17},{17,25},{25,1},{2,10},{10... | collective-permute-start | bytes 393224 | tf_op jit(solution)/shard_map/ppermute | solution.py:334
  (13 other events, 17.3 us)
